TPU v7x, 256 devices: a whole 4x4x8 slice. The times are simulated.
256 devices in a mesh: sp: 16 (over y, x), tp: 16 (over z, core).
Axes of the slice: x: 4, y: 4, z: 8, core: 2. Of those that a mesh axis runs over, the one named last changes fastest.
Arguments:
- residual_in: bfloat16 [8192, 4096], P('sp', 'tp'), may hold values from -24 to 24
- norm_gain: float32 [2, 4096], replicated, may hold values from 0.1 to 1.9
- gate_proj: bfloat16 [2, 4096, 2048], P(None, 'sp', 'tp'), may hold values from -0.09375 to 0.09375
- filter_proj: bfloat16 [2, 4096, 2048], P(None, 'sp', 'tp'), may hold values from -0.09375 to 0.09375
- signal_proj: bfloat16 [2, 4096, 2048], P(None, 'sp', 'tp'), may hold values from -0.09375 to 0.09375
- conv_taps: float32 [2, 3, 2048], P(None, None, 'tp'), may hold values from -3 to 3
- out_proj: bfloat16 [2, 2048, 4096], P(None, 'tp', 'sp'), may hold values from -0.1875 to 0.1875
- final_gain: float32 [4096], P('tp'), may hold values from 0.1 to 1.9
Outputs:
- final_rows: float32 [8192, 4096], P('sp', 'tp')
All inputs are finite; a program needn't handle non-finite values.
Results may differ from a plain program's by a relative error of at most 0.033.
Values may be sent and summed in bfloat16 or wider, within the bound.
A program may use at most 64 MiB of HBM per device.

v0:
```python
import jax
import jax.numpy as jnp
from jax import lax
from jax.sharding import PartitionSpec as P

D = 4096
TAPS = 3
LAYERS = 2


norm_floor = 1e-06


def rows_first(arrays, axis, dims):
    turned = [jnp.moveaxis(a, dim, 0) for a, dim in zip(arrays, dims)]
    both = jnp.concatenate([t.reshape(len(t), -1) for t in turned], axis=1)
    result, at, outs = (lax.all_gather(both, axis, axis=0, tiled=True), 0, [])
    for t, dim in zip(turned, dims):
        share = result[:, at : at + t[0].size].reshape(-1, *t.shape[1:])
        outs.append(jnp.moveaxis(share, 0, dim))
        at += t[0].size
    return tuple(outs)


def from_behind(value, axis, steps):
    count = lax.axis_size(axis)
    initial, last = (max(0, -steps), min(count, count - steps))
    return lax.ppermute(value, axis, [(source, source + steps) for source in range(initial, last)])


def filled_up(lines, count):
    spare = -lines.shape[0] % count
    if not spare:
        return lines
    return jnp.concatenate([lines, jnp.zeros((spare, *lines.shape[1:]), lines.dtype)])


def total_of(array, axis):
    lines = array.reshape(-1, *array.shape[1:][-1:])
    own = lax.psum_scatter(
        filled_up(lines, lax.axis_size(axis)), axis, scatter_dimension=0, tiled=True
    )
    whole = lax.all_gather(own, axis).reshape(-1, *lines.shape[1:])
    return lax.slice_in_dim(whole, 0, len(lines)).reshape(array.shape)


def sent_to_all(array, axis):
    count = lax.axis_size(axis)
    return lax.all_to_all(
        jnp.broadcast_to(array[None], (count, *array.shape)), axis, 0, 0, tiled=True
    )


def over_copies(array, axis):
    return sent_to_all(array, axis).sum(axis=0)


def rms_scaled(values, gain_row):
    mean_square = jnp.mean(values * values, axis=-1, keepdims=True)
    return values * lax.rsqrt(mean_square + norm_floor) * gain_row


def stored(values):
    return lax.optimization_barrier(values.astype(jnp.bfloat16)).astype(jnp.float32)


def per_device(
    residual_in, norm_gain, gate_proj, filter_proj, signal_proj, conv_taps, out_proj, final_gain
):
    own_cols = residual_in.shape[1]
    whole_gate, whole_filter, whole_signal, whole_out = rows_first(
        (gate_proj, filter_proj, signal_proj, out_proj), "sp", (1, 1, 1, 2)
    )

    def mix_layer(full_rows, layer_number):
        normed = rms_scaled(full_rows.astype(jnp.float32), norm_gain[layer_number]).astype(
            jnp.bfloat16
        )
        gate_sum = jnp.dot(normed, whole_gate[layer_number], preferred_element_type=jnp.float32)
        filter_sum = jnp.dot(normed, whole_filter[layer_number], preferred_element_type=jnp.float32)
        signal_sum = jnp.dot(normed, whole_signal[layer_number], preferred_element_type=jnp.float32)
        gate_rows = stored(gate_sum)
        product = (stored(filter_sum) * stored(signal_sum)).astype(jnp.bfloat16)
        span_rows = product.shape[0]
        edge_rows = from_behind(product[span_rows - (TAPS - 1) :], "sp", 1)
        extended = jnp.concatenate([edge_rows, product], axis=0)
        filtered = jnp.zeros(product.shape, jnp.float32)
        for tap_index in range(TAPS):
            filtered = filtered + conv_taps[layer_number, tap_index] * extended[
                tap_index : tap_index + span_rows
            ].astype(jnp.float32)
        return (gate_rows * filtered).astype(jnp.bfloat16)

    def project_out(mixed_rows, layer_number):
        return jnp.dot(mixed_rows, whole_out[layer_number], preferred_element_type=jnp.float32)

    full_rows = lax.all_gather(residual_in, "tp", axis=1, tiled=True)
    layer_number = 0
    branch_all = total_of(
        project_out(mix_layer(full_rows, layer_number), layer_number).astype(jnp.bfloat16), "tp"
    ).astype(jnp.float32)
    full_rows = (full_rows.astype(jnp.float32) + branch_all).astype(jnp.bfloat16)
    last_branch = lax.psum_scatter(
        project_out(mix_layer(full_rows, LAYERS - 1), LAYERS - 1).astype(jnp.bfloat16),
        "tp",
        scatter_dimension=1,
        tiled=True,
    ).astype(jnp.float32)
    own_rows = lax.dynamic_slice_in_dim(full_rows, lax.axis_index("tp") * own_cols, own_cols, 1)
    stream = (own_rows.astype(jnp.float32) + last_branch).astype(jnp.bfloat16)
    stream_float = stream.astype(jnp.float32)
    square_sum = over_copies(jnp.sum(stream_float * stream_float, axis=1, keepdims=True), "tp")
    return stream_float * lax.rsqrt(square_sum / D + norm_floor) * final_gain


def solution(mesh):
    return jax.shard_map(
        per_device,
        mesh=mesh,
        in_specs=(
            P("sp", "tp"),
            P(),
            P(None, "sp", "tp"),
            P(None, "sp", "tp"),
            P(None, "sp", "tp"),
            P(None, None, "tp"),
            P(None, "tp", "sp"),
            P("tp"),
        ),
        out_specs=P("sp", "tp"),
        check_vma=False,
    )
```

profile of v0, /device:TPU:1, one launch (start us, length us, event | category | flops | bytes accessed | tf_op | source)
XLA Modules:
  0.0 371.2 jit_solution(10895303334797916029)
XLA Ops:
  6.5 0.7 all-gather.5.cloned.1.call-update
  7.3 0.0 all-gather.7.cloned.1.call-start
  7.3 1.0 copy.14
  8.3 1.0 copy.13
  9.3 1.0 copy.12
  10.3 1.7 pad_maximum_fusion
  12.1 0.0 all-gather.7.cloned.1.call-update
  12.1 0.0 reduce-scatter.3.cloned.1.call-start
  12.2 0.8 slice_bitcast_fusion.18
  12.9 0.9 fusion.23
  13.8 48.8 %all-gather.5.cloned.1.call-done = bf16[512,4096]{1,0:T(8,128)(2,1)} async-done(((bf16[512,256]{1,0:T(8,128)(2,1)}), bf16[512,4096]{1,0:T(8,128)(2,1)}) %all-gather.5.cloned.1.call-update) | async-done | bytes 4194320 | tf_op jit(solution)/shard_map/all_gather | solution.py:97
  62.6 3.2 fusion.3
  65.8 0.2 copy-done
  66.1 3.6 fusion.5
  69.6 74.2 %all-gather.7.cloned.1.call-done = bf16[4096,1024]{0,1:T(8,128)(2,1)} async-done(((bf16[256,1024]{0,1:T(8,128)(2,1)}), bf16[4096,1024]{0,1:T(8,128)(2,1)}) %all-gather.7.cloned.1.call-update) | async-done | bytes 8388624 | tf_op jit(solution)/shard_map/all_gather | solution.py:17
  143.8 4.0 %fusion.22 = (bf16[4096,256]{0,1:T(8,128)(2,1)S(1)}, bf16[4096,256]{0,1:T(8,128)(2,1)S(1)}, bf16[4096,256]{0,1:T(8,128)(2,1)S(1)}, bf16[4096,256]{0,1:T(8,128)(2,1)S(1)}) fusion(bf16[4096,1024]{0,1:T(8,128)(2,1)} %all-gather.7.cloned.1.call-done), kind=kLoop, calls=%fused_computation.65 | loop fusion | bytes 16777216 | tf_op jit(solution)/shard_map/slice | solution.py:19
  147.8 0.0 copy-start.5
  147.8 0.0 copy-start.7
  147.8 0.0 copy-start.3
  147.8 0.6 copy-done.2
  148.4 1.2 convolution_convert_fusion.5
  149.7 1.3 convolution_convert_fusion.6
  151.0 2.8 collective-permute-start
  153.8 1.2 convolution_convert_fusion.7
  155.1 0.0 collective-permute-done
  155.1 3.2 convolution_convert_fusion.1
  158.3 0.0 reduce-scatter.3.cloned.1.call-update
  158.3 0.0 all-gather.9.cloned.1.call-start
  158.4 63.4 %reduce-scatter.3.cloned.1.call-done = bf16[32,4096]{1,0:T(8,128)(2,1)} async-done(((bf16[512,4096]{1,0:T(8,128)(2,1)}), bf16[32,4096]{1,0:T(8,128)(2,1)}) %reduce-scatter.3.cloned.1.call-update) | async-done | bytes 262160 | tf_op jit(solution)/shard_map/reduce_scatter | solution.py:40
  221.8 0.0 all-gather.9.cloned.1.call-update
  221.8 0.2 reduce-scatter.5.cloned.1.call-start
  222.1 45.3 %all-gather.9.cloned.1.call-done = bf16[512,4096]{1,0:T(8,128)(2,1)} async-done(((bf16[32,4096]{1,0:T(8,128)(2,1)}), bf16[512,4096]{1,0:T(8,128)(2,1)}) %all-gather.9.cloned.1.call-update) | async-done | bytes 4194320 | tf_op jit(solution)/shard_map/all_gather | solution.py:43
  267.4 5.5 %fusion = (f32[512]{0:T(512)S(1)}, bf16[512,4096]{1,0:T(8,128)(2,1)S(1)}) fusion(bf16[512,4096]{1,0:T(8,128)(2,1)} %all-gather.9.cloned.1.call-done, bf16[512,4096]{1,0:T(8,128)(2,1)} %all-gather.5.cloned.1.call-done), kind=kLoop, calls=%fused_computation.5 | loop fusion | flops 14679552 | bytes 12584960 | tf_op jit(solution)/shard_map/reduce_sum | solution.py:59
  272.9 1.6 fusion.2
  274.5 0.5 copy-done.1
  275.0 1.0 copy-done.8
  276.0 1.2 convolution_convert_fusion.2
  277.2 0.3 copy-done.6
  277.6 1.2 convolution_convert_fusion.3
  278.9 3.1 collective-permute-start.1
  282.0 1.3 convolution_convert_fusion.4
  283.3 0.0 collective-permute-done.1
  283.3 3.2 convolution_convert_fusion
  286.5 0.0 reduce-scatter.5.cloned.1.call-update
  286.6 59.8 %reduce-scatter.5.cloned.1.call-done = bf16[512,256]{1,0:T(8,128)(2,1)} async-done(((bf16[512,4096]{1,0:T(8,128)(2,1)}), bf16[512,256]{1,0:T(8,128)(2,1)}) %reduce-scatter.5.cloned.1.call-update) | async-done | bytes 262160 | tf_op jit(solution)/shard_map/reduce_scatter | solution.py:103
  346.3 1.2 fusion.7
  347.5 15.2 %all_to_all.5 = f32[16,512,1]{1,2,0:T(1,128)S(1)} all-to-all(f32[16,512,1]{1,2,0:T(1,128)S(1)} %broadcast_in_dim.2), channel_id=1, replica_groups=mesh['sp'=16,'tp'=16] {'tp'}, dimensions={0} | all-to-all | bytes 65536 | tf_op jit(solution)/shard_map/all_to_all | solution.py:49
  362.7 2.0 fusion.8
  (22 shorter events, 0.2 us)
Async XLA Ops:
  6.5 56.1 %all-gather.5.cloned.1.call-start = ((), (), s32[]{:S(2)}) async-start(), calls=%async_computation.3 | async-start | bytes 4456448 | tf_op jit(solution)/shard_map/all_gather | solution.py:97
  7.3 136.5 %all-gather.7.cloned.1.call-start = ((), (), s32[]{:S(2)}) async-start(), calls=%async_computation.4 | async-start | bytes 8912896 | tf_op jit(solution)/shard_map/all_gather | solution.py:17
  12.1 209.7 %reduce-scatter.3.cloned.1.call-start = ((), (), s32[]{:S(2)}) async-start(), calls=%async_computation.5 | async-start | bytes 4456448 | tf_op jit(solution)/shard_map/reduce_scatter | solution.py:40
  62.6 3.4 copy-start
  143.8 4.7 %copy-start.2 = (bf16[512,4096]{1,0:T(8,128)(2,1)S(1)}, bf16[512,4096]{1,0:T(8,128)(2,1)}, u32[]{:S(2)}) copy-start(bf16[512,4096]{1,0:T(8,128)(2,1)} %fusion.5) | copy-start | bytes 12582916
  147.8 3.1 copy-start.5
  147.8 3.1 copy-start.7
  147.8 6.0 %copy-start.3 = (bf16[4096,256]{0,1:T(8,128)(2,1)}, bf16[4096,256]{0,1:T(8,128)(2,1)S(1)}, u32[]{:S(2)}) copy-start(bf16[4096,256]{0,1:T(8,128)(2,1)S(1)} %get-tuple-element.7) | copy-start | bytes 6291460
  151.0 4.1 %collective-permute-start = (bf16[2,128]{1,0:T(2,128)(2,1)S(1)}, bf16[2,128]{1,0:T(2,128)(2,1)S(1)}, u32[]{:S(2)}, u32[]{:S(2)}) collective-permute-start(bf16[2,128]{1,0:T(2,128)(2,1)S(1)} %slice.110), channel_id=1, source_target_pairs={{0,16},{16,32},{32,48},{48,64},{64,80},{80,96},{96,112},{112,128},... | collective-permute-start | bytes 1544 | tf_op jit(solution)/shard_map/ppermute | solution.py:28
  158.3 109.0 %all-gather.9.cloned.1.call-start = ((), (), s32[]{:S(2)}) async-start(), calls=%async_computation.7 | async-start | bytes 4456448 | tf_op jit(solution)/shard_map/all_gather | solution.py:43
  221.8 124.5 %reduce-scatter.5.cloned.1.call-start = ((), (), s32[]{:S(2)}) async-start(), calls=%async_computation.6 | async-start | bytes 4456448 | tf_op jit(solution)/shard_map/reduce_scatter | solution.py:103
  272.8 2.1 copy-start.1
  272.9 3.1 copy-start.8
  276.0 1.6 copy-start.6
  277.6 4.4 %copy-start.4 = (bf16[4096,256]{0,1:T(8,128)(2,1)S(1)}, bf16[4096,256]{0,1:T(8,128)(2,1)}, u32[]{:S(2)}) copy-start(bf16[4096,256]{0,1:T(8,128)(2,1)} %copy-done.3) | copy-start | bytes 6291460
  278.9 4.4 %collective-permute-start.1 = (bf16[2,128]{1,0:T(2,128)(2,1)S(1)}, bf16[2,128]{1,0:T(2,128)(2,1)S(1)}, u32[]{:S(2)}, u32[]{:S(2)}) collective-permute-start(bf16[2,128]{1,0:T(2,128)(2,1)S(1)} %slice.118), channel_id=1, source_target_pairs={{0,16},{16,32},{32,48},{48,64},{64,80},{80,96},{96,112},{112,128},... | collective-permute-start | bytes 1544 | tf_op jit(solution)/shard_map/ppermute | solution.py:28
  286.5 76.2 %copy-start.9 = (f32[256]{0:T(256)S(1)}, f32[256]{0:T(256)}, u32[]{:S(2)}) copy-start(f32[256]{0:T(256)} %param.15) | copy-start | bytes 3076
Sparse Core Ops, SparseCore 0:
  9.1 53.4 all-gather.4
  65.0 78.7 all-gather.6
  158.5 63.2 reduce-scatter.2
  223.5 43.8 all-gather.8
  286.7 59.5 reduce-scatter.4
where the time goes:
time: 372 us; the launch traced here: 371 us
  waiting for transfers between devices  292 us (78%)
  other arithmetic  18.9 us (5%)
  blocking collectives  15.2 us (4%)
  matrix products  14 us (4%)
  between operations  13.4 us (4%)
  local copies, waits for them, and re-layouts  11.4 us (3%)
  starting transfers between devices  6.25 us (2%)
    all_gather x1, waiting for transfers between devices, rows_first(): result, at, outs = (lax.all_gather(both, axis, axis=0, tiled=True), 0, [])  74.2 us
    reduce_scatter x1, waiting for transfers between devices, total_of(): lax.psum_scatter(filled_up(lines, lax.axis_size(axis)), axis, scatter_dim...  63.4 us
    reduce_scatter x1, waiting for transfers between devices, per_device(): lax.psum_scatter(project_out(mix_layer(full_rows, LAYERS - 1), LAYERS - 1...  59.8 us
    all_gather x1, waiting for transfers between devices, per_device(): full_rows = lax.all_gather(residual_in, 'tp', axis=1, tiled=True)  48.8 us
    all_gather x1, waiting for transfers between devices, total_of(): whole = lax.all_gather(own, axis).reshape(-1, *lines.shape[1:])  45.3 us
    all_to_all x1, blocking collectives, sent_to_all(): lax.all_to_all(jnp.broadcast_to(array[None], (count, *array.shape)), axis...  15.2 us
    reduce_sum x2, other arithmetic, rms_scaled(): mean_square = jnp.mean(values * values, axis=-1, keepdims=True)  8.68 us
  transfers between devices with their start and end apart: 7, of which 5 were waited for; matrix products, arithmetic and copies ran while one was open for 4% of the time, Pallas kernels for 0%

commit v1 on v0

v1 whole, which is shorter than its diff:
```python
import jax
import jax.numpy as jnp
from jax import lax
from jax.experimental import pallas as pl
from jax.experimental.pallas import tpu as pltpu
from jax.sharding import PartitionSpec as P

D = 4096
TAPS = 3
LAYERS = 2
FLOOR = 1e-06

NZ = 8
SIDE = 4
ROWS = 256
PIECE = 512
CH = 128
WIDE = 512
NQ = 2
QR = ROWS // NQ

F32 = jnp.float32
BF16 = jnp.bfloat16
MESH = pl.DeviceIdType.MESH


def aligned(index, size):
    return pl.ds(pl.multiple_of(index * size, size), size)


def kernel(
    res, norm_gain, gate, filt, sig, taps, outp, final_gain, out,
    x_all, xg, w_all, w_out, acc, prod, mixed, sq, rs_out, rs_in, halo, tap_all, sums, st, fin_out, fin_in,
    ag_s, ag_r, w_s, w_r, d_s, d_r, rs_s, rs_r, h_s, h_r, s_s, s_r, m_s, m_r,
):
    s = lax.axis_index("sp")
    t = lax.axis_index("tp")
    z, c = t // 2, t % 2
    y, x = s // SIDE, s % SIDE
    other = 1 - c
    partner = (s, 2 * z + other)

    def at_z(k):
        return (s, ((z + k) % NZ) * 2 + c)

    def at_x(k):
        return (y * SIDE + (x + k) % SIDE, t)

    def at_y(k):
        return (((y + k) % SIDE) * SIDE + x, t)

    halo_next = ((s + c) % 16, 2 * z + other)
    halo_far = ((s + 2 * c + 15) % 16, 2 * z + other)

    def rdma(src, dst, send, recv, device):
        return pltpu.make_async_remote_copy(
            src_ref=src, dst_ref=dst, send_sem=send, recv_sem=recv, device_id=device, device_id_type=MESH
        )

    pending = []

    def start(copy):
        copy.start()
        pending.append(copy)

    barrier = pltpu.get_barrier_semaphore()
    peers = [at_z(k) for k in range(1, NZ)] + [at_x(1), at_x(-1), at_y(1), at_y(-1), partner, halo_far]
    for peer in peers:
        pl.semaphore_signal(barrier, inc=1, device_id=peer, device_id_type=MESH)

    own_cols = aligned(c, 256)
    own_rows = aligned(c, ROWS)
    other_rows = aligned(other, ROWS)
    own_wide = aligned(c, WIDE)

    x_all[0, z, :, own_cols] = res[own_rows, :]
    for l in range(LAYERS):
        for part, ref in enumerate((gate, filt, sig)):
            w_all[l, aligned(s, 256), pl.ds(pl.multiple_of(c * WIDE + part * CH, CH), CH)] = ref[l]
        for h in range(2):
            w_all[l, aligned(2 * s + h, CH), pl.ds(pl.multiple_of(c * WIDE + 3 * CH, CH), CH)] = outp[
                l, :, h * CH : (h + 1) * CH
            ]
    for l in range(LAYERS):
        for k in range(TAPS):
            tap_all[c, l * TAPS + k] = taps[l, k : k + 1, :]
    pl.semaphore_wait(barrier, len(peers))

    start(rdma(res.at[other_rows, :], x_all.at[0, z, :, own_cols], m_s.at[0], m_r.at[0], partner))
    start(rdma(tap_all.at[c], tap_all.at[c], m_s.at[1], m_r.at[1], partner))

    def piece(l, axis, along, across, lo, size):
        if axis == 0:
            yy, xx = y + across, x + along
        else:
            yy, xx = y + along, x + across
        index = ((yy + SIDE) % SIDE) * SIDE + (xx + SIDE) % SIDE
        return w_all.at[l, pl.ds(pl.multiple_of(index * 256 + lo, 64), size), own_wide]

    def w_copy(l, group, half, axis, across, sign, fwd, sending):
        step = sign if fwd else 0
        along = -step if sending else -step - sign
        lo, size = half * 128, 128
        if fwd:
            lo, size = lo + (0 if sign == 1 else 64), 64
        slot = group * 4 + (2 if fwd else 0) + (0 if sign == 1 else 1)
        ref = piece(l, axis, along, across, lo, size)
        device = at_x(sign) if axis == 0 else at_y(sign)
        return rdma(ref, ref, w_s.at[l, slot], w_r.at[l, slot], device)

    groups = {("a", 1): (0, 0, 0, 0), ("b", 1): (5, 1, 1, 0)}
    for i, p in enumerate((0, -1, 1, 2)):
        groups["a", 2, p] = (1 + i, 0, 1, p)
        groups["b", 2, p] = (6 + i, 1, 0, p)

    def w_send(l, *name):
        group, half, axis, across = groups[name]
        for sign in (1, -1):
            start(w_copy(l, group, half, axis, across, sign, False, True))

    def w_forward(l, *name):
        group, half, axis, across = groups[name]
        for sign in (1, -1):
            w_copy(l, group, half, axis, across, sign, False, False).wait_recv()
            start(w_copy(l, group, half, axis, across, sign, True, True))

    def w_finish(l, *name):
        group, half, axis, across = groups[name]
        for sign in (1, -1):
            w_copy(l, group, half, axis, across, sign, True, False).wait_recv()

    def w_row(l, k, core):
        return w_all.at[l, aligned((y + k + SIDE) % SIDE, 1024), aligned(core, WIDE)]

    def w_hand(l, k):
        slot = (k + SIDE) % SIDE
        start(rdma(w_row(l, k, c), w_row(l, k, c), d_s.at[l, slot], d_r.at[l, slot], partner))

    def w_taken(l, k):
        slot = (k + SIDE) % SIDE
        rdma(w_row(l, k, other), w_row(l, k, other), d_s.at[l, slot], d_r.at[l, slot], partner).wait_recv()

    def w_stage(l, stage):
        if stage == 0:
            w_send(l, "a", 1)
            w_send(l, "b", 1)
            w_send(l, "b", 2, 0)
            w_send(l, "a", 2, 0)
        elif stage == 1:
            w_forward(l, "a", 1)
            w_forward(l, "b", 1)
            for p in (-1, 1):
                w_send(l, "a", 2, p)
                w_send(l, "b", 2, p)
        elif stage == 2:
            w_forward(l, "b", 2, 0)
            w_forward(l, "a", 2, 0)
            w_finish(l, "a", 1)
            w_send(l, "a", 2, 2)
            w_finish(l, "b", 1)
            w_send(l, "b", 2, 2)
        elif stage == 3:
            for p in (-1, 1):
                w_forward(l, "a", 2, p)
                w_forward(l, "b", 2, p)
            w_finish(l, "a", 2, 0)
            w_finish(l, "b", 2, 0)
            w_hand(l, 0)
        elif stage == 4:
            w_forward(l, "a", 2, 2)
            w_forward(l, "b", 2, 2)
            for p in (-1, 1):
                w_finish(l, "a", 2, p)
                w_finish(l, "b", 2, p)
            w_hand(l, -1)
            w_hand(l, 1)
        elif stage == 5:
            w_finish(l, "a", 2, 2)
            w_finish(l, "b", 2, 2)
            w_hand(l, 2)
        else:
            for k in (0, -1, 1, 2):
                w_taken(l, k)

    def build_w_out(l):
        def body(i, carry):
            for core in range(2):
                w_out[core * CH : (core + 1) * CH, aligned(i, CH)] = w_all[
                    l, aligned(i, CH), core * WIDE + 3 * CH : (core + 1) * WIDE
                ]
            return carry

        lax.fori_loop(0, D // CH, body, 0)

    def ag_has(way, dist, q):
        return dist < 3 or (q < NQ // 2) == (way == 0)

    def ag_copy(l, way, dist, q, sending):
        sign = 1 - 2 * way
        chunk = (z - sign * (dist if sending else dist + 1) + NZ) % NZ
        ref = x_all.at[l, chunk, pl.ds(q * QR, QR), :]
        return rdma(ref, ref, ag_s.at[l, way, dist * NQ + q], ag_r.at[l, way, dist * NQ + q], at_z(sign))

    def ag_send(l, dist, q):
        for way in range(2):
            if ag_has(way, dist, q):
                start(ag_copy(l, way, dist, q, True))

    def ag_step(l, dist, q):
        for way in range(2):
            if ag_has(way, dist, q):
                ag_copy(l, way, dist, q, False).wait_recv()
                if dist < 3 and ag_has(way, dist + 1, q):
                    start(ag_copy(l, way, dist + 1, q, True))

    def take(l, chunk):
        value = x_all[l, chunk].astype(F32)
        square = value * value
        total = square[:, :128]
        for i in range(1, PIECE // 128):
            total = total + square[:, i * 128 : (i + 1) * 128]
        sq[...] += total
        xg[chunk] = (value * norm_gain[l : l + 1, aligned(chunk, PIECE)]).astype(BF16)

    def multiply(l, chunk):
        rows = aligned(chunk, PIECE)
        for core in range(2):
            cols = pl.ds(core * 3 * CH, 3 * CH)
            acc[:, cols] += jnp.dot(
                xg[chunk], w_all[l, rows, core * WIDE : core * WIDE + 3 * CH], preferred_element_type=F32
            )

    def start_sums():
        sq[...] = jnp.zeros_like(sq)
        acc[...] = jnp.zeros_like(acc)

    def chunk_at(k):
        return (z + k + NZ) % NZ

    def mix(l, lo, size):
        rows = pl.ds(lo, size)
        for core in range(2):
            cols = pl.ds(core * CH, CH)
            filtered = jnp.zeros((size, CH), F32)
            for k in range(TAPS):
                filtered = filtered + tap_all[core, l * TAPS + k] * prod[pl.ds(8 + lo - (TAPS - 1) + k, size), cols]
            gated = acc[rows, core * 3 * CH : core * 3 * CH + CH]
            mixed[rows, cols] = (gated * filtered).astype(BF16)

    def gates(l):
        mean = jnp.sum(sq[...], axis=1, keepdims=True) / D
        scale = lax.rsqrt(mean + FLOOR)
        for core in range(2):
            base = core * 3 * CH
            value = (acc[:, base + CH : base + 2 * CH] * scale) * (acc[:, base + 2 * CH : base + 3 * CH] * scale)
            prod[8:, core * CH : (core + 1) * CH] = value.astype(BF16).astype(F32)
            acc[:, base : base + CH] = acc[:, base : base + CH] * scale
        halo[l, 0] = prod[ROWS:, :]

    def halo_copy(l):
        return rdma(halo.at[l, 0], halo.at[l, 1], h_s.at[l], h_r.at[l], halo_next)

    def take_halo(l):
        halo_copy(l).wait_recv()
        first = jnp.logical_and(s == 0, c == 0)
        prod[:8, :] = jnp.where(first, 0.0, halo[l, 1])

    def rs_has(way, k, q):
        return k < 4 or (q < NQ // 2) == (way == 0)

    def rs_copy(l, way, k, q):
        slot = (k - 1) * NQ + q
        return rdma(
            rs_out.at[l, way, slot], rs_in.at[l, way, slot], rs_s.at[l, way, slot], rs_r.at[l, way, slot],
            at_z(1 - 2 * way),
        )

    def partial(q, chunk):
        return jnp.dot(mixed[q * QR : (q + 1) * QR, :], w_out[:, aligned(chunk, PIECE)], preferred_element_type=F32)

    def arrived(l, way, k, q):
        rs_copy(l, way, k, q).wait_recv()
        return rs_in[l, way, (k - 1) * NQ + q].astype(F32)

    def rs_step(l, i, q):
        for way in range(2):
            k = 4 - i if rs_has(way, 4, q) else 3 - i
            if k < 1:
                continue
            value = partial(q, chunk_at(k * (1 - 2 * way)))
            if i > 0:
                value = value + arrived(l, way, k + 1, q)
            rs_out[l, way, (k - 1) * NQ + q] = value.astype(BF16)
            start(rs_copy(l, way, k, q))

    def rs_last(l, q):
        value = partial(q, z)
        for way in range(2):
            value = value + arrived(l, way, 1, q)
        return (x_all[l, z, pl.ds(q * QR, QR), :].astype(F32) + value).astype(BF16)

    upper = list(range(NQ // 2, NQ))
    lower = list(range(NQ // 2))

    start_sums()
    rdma(res.at[other_rows, :], x_all.at[0, z, :, aligned(other, 256)], m_s.at[0], m_r.at[0], partner).wait_recv()
    for q in range(NQ):
        ag_send(0, 0, q)
    w_stage(0, 0)
    take(0, z)
    for dist in range(4):
        for q in range(NQ):
            ag_step(0, dist, q)
            if q == NQ // 2 - 1:
                w_stage(0, (1, 1, 3, 4)[dist]) if dist != 1 else None
        if dist == 0:
            w_stage(0, 2)
        if dist < 3:
            take(0, chunk_at(-dist - 1))
            take(0, chunk_at(dist + 1))
        else:
            take(0, chunk_at(4))
    w_stage(0, 5)
    w_stage(1, 0)
    rdma(tap_all.at[other], tap_all.at[other], m_s.at[1], m_r.at[1], partner).wait_recv()
    w_stage(0, 6)

    def all_blocks(i, carry):
        multiply(0, i)
        return carry

    lax.fori_loop(0, NZ, all_blocks, 0)

    for l in range(LAYERS):
        gates(l)
        start(halo_copy(l))
        build_w_out(l)
        mix(l, ROWS // 2, ROWS // 2)
        for i in range(4):
            for q in upper:
                rs_step(l, i, q)
            if i == 0:
                take_halo(l)
                mix(l, 0, ROWS // 2)
            for q in lower:
                rs_step(l, i, q)
            if l == 0:
                w_stage(1, 1 + i)
        if l == 0:
            start_sums()
            for q in upper + lower:
                x_all[1, z, pl.ds(q * QR, QR), :] = rs_last(0, q)
                ag_send(1, 0, q)
            w_stage(1, 5)
            take(1, z)
            w_stage(1, 6)
            multiply(1, z)
            for dist in range(4):
                for q in upper + lower:
                    ag_step(1, dist, q)
                for k in (-dist - 1, dist + 1) if dist < 3 else (4,):
                    take(1, chunk_at(k))
                    multiply(1, chunk_at(k))

    for q in upper + lower:
        value = rs_last(1, q).astype(F32)
        st[pl.ds(q * QR, QR), :] = value
    value = st[...]
    square = jnp.sum(value * value, axis=1, keepdims=True)
    sums[z] = jnp.broadcast_to(square, (ROWS, 128)).T[:8, :]

    def sums_copy(k, sending):
        ref = sums.at[z if sending else chunk_at(-k)]
        return rdma(ref, ref, s_s.at[k], s_r.at[k], at_z(k))

    for k in (4, 3, 5, 2, 6, 1, 7):
        start(sums_copy(k, True))
    total = sums[z]
    for k in (1, 7, 2, 6, 3, 5, 4):
        sums_copy(k, False).wait_recv()
        total = total + sums[chunk_at(-k)]
    total = jnp.broadcast_to(total[:1, :], (128, ROWS)).T[:, :1]
    scale = lax.rsqrt(total / D + FLOOR)
    fin_out[...] = st[:, aligned(other, 256)] * scale
    back = rdma(fin_out, fin_in, m_s.at[2], m_r.at[2], partner)
    start(back)
    out[own_rows, :] = st[:, own_cols] * scale * final_gain[...]
    back.wait_recv()
    out[other_rows, :] = fin_in[...] * final_gain[...]
    for copy in pending:
        copy.wait_send()


def per_device(residual_in, norm_gain, gate_proj, filter_proj, signal_proj, conv_taps, out_proj, final_gain):
    vmem = pl.BlockSpec(memory_space=pltpu.VMEM)
    dma = pltpu.SemaphoreType.DMA
    return pl.pallas_call(
        kernel,
        out_shape=jax.ShapeDtypeStruct((2 * ROWS, 256), F32),
        in_specs=[vmem] * 8,
        out_specs=vmem,
        scratch_shapes=[
            pltpu.VMEM((LAYERS, NZ, ROWS, PIECE), BF16),
            pltpu.VMEM((NZ, ROWS, PIECE), BF16),
            pltpu.VMEM((LAYERS, D, 2 * WIDE), BF16),
            pltpu.VMEM((2 * CH, D), BF16),
            pltpu.VMEM((ROWS, 6 * CH), F32),
            pltpu.VMEM((8 + ROWS, 2 * CH), F32),
            pltpu.VMEM((ROWS, 2 * CH), BF16),
            pltpu.VMEM((ROWS, 128), F32),
            pltpu.VMEM((LAYERS, 2, 4 * NQ, QR, PIECE), BF16),
            pltpu.VMEM((LAYERS, 2, 4 * NQ, QR, PIECE), BF16),
            pltpu.VMEM((LAYERS, 2, 8, 2 * CH), F32),
            pltpu.VMEM((2, LAYERS * TAPS, 1, CH), F32),
            pltpu.VMEM((NZ, 8, ROWS), F32),
            pltpu.VMEM((ROWS, PIECE), F32),
            pltpu.VMEM((ROWS, 256), F32),
            pltpu.VMEM((ROWS, 256), F32),
            dma((LAYERS, 2, 4 * NQ)), dma((LAYERS, 2, 4 * NQ)),
            dma((LAYERS, 40)), dma((LAYERS, 40)),
            dma((LAYERS, SIDE)), dma((LAYERS, SIDE)),
            dma((LAYERS, 2, 4 * NQ)), dma((LAYERS, 2, 4 * NQ)),
            dma((LAYERS,)), dma((LAYERS,)),
            dma((NZ,)), dma((NZ,)),
            dma((3,)), dma((3,)),
        ],
        compiler_params=pltpu.CompilerParams(
            collective_id=0, has_side_effects=True, vmem_limit_bytes=58 * 1024 * 1024
        ),
    )(
        residual_in, norm_gain, gate_proj, filter_proj, signal_proj, conv_taps, out_proj,
        final_gain.reshape(1, -1),
    )


def solution(mesh):
    return jax.shard_map(
        per_device,
        mesh=mesh,
        in_specs=(
            P("sp", "tp"),
            P(),
            P(None, "sp", "tp"),
            P(None, "sp", "tp"),
            P(None, "sp", "tp"),
            P(None, None, "tp"),
            P(None, "tp", "sp"),
            P("tp"),
        ),
        out_specs=P("sp", "tp"),
        check_vma=False,
    )
```

time: 372 us -> 129 us (0.35)
  waiting for transfers between devices: 292 us -> 0 us
  Pallas kernels: 0 us -> 126 us
  other arithmetic: 18.9 us -> 0 us
  blocking collectives: 15.2 us -> 0 us
  matrix products: 14 us -> 0 us
  between operations: 13.4 us -> 0.01 us
  local copies, waits for them, and re-layouts: 11.4 us -> 3.15 us
  starting transfers between devices: 6.25 us -> 0 us
    all_gather x3 -> x0, waiting for transfers between devices: 168 us -> none  [the longest x1 74.2 us: rows_first(): result, at, outs = (lax.all_gather(both, axis, axis=0, tiled=True), 0, [])]
    pallas_call x0 -> x1, Pallas kernels: none -> 126 us  [per_device(): pl.pallas_call(kernel, out_shape=jax.ShapeDtypeStruct((2 * ROWS, 256), F3...]
    reduce_scatter x2 -> x0, waiting for transfers between devices: 123 us -> none  [the longest x1 63.4 us: total_of(): lax.psum_scatter(filled_up(lines, lax.axis_size(axis)), axis, scatter_dim...]
    all_to_all x1 -> x0, blocking collectives: 15.2 us -> none  [sent_to_all(): lax.all_to_all(jnp.broadcast_to(array[None], (count, *array.shape)), axis...]
    dot_general x8 -> x0, matrix products: 14 us -> none  [the longest x2 6.45 us: project_out(): jnp.dot(mixed_rows, whole_out[layer_number], preferred_element_type=jnp.f...]
    reduce_sum x4 -> x0, other arithmetic: 9.91 us -> none  [the longest x2 8.68 us: rms_scaled(): mean_square = jnp.mean(values * values, axis=-1, keepdims=True)]
    ppermute x2 -> x0, starting transfers between devices: 5.91 us -> none  [from_behind(): lax.ppermute(value, axis, [(source, source + steps) for source in range(i...]
    convert_element_type x4 -> x0, other arithmetic: 5.24 us -> none  [the longest x2 5.16 us: mix_layer(): rms_scaled(full_rows.astype(jnp.float32), norm_gain[layer_number])]
  transfers between devices with their start and end apart: 7 -> 0, of which waited for: 5 -> 0; matrix products, arithmetic and copies ran while one was open for 4% -> 0% of each run, Pallas kernels for 0% -> 0%
where the time goes in v1:
time: 129 us
  Pallas kernels  126 us (98%)
  local copies, waits for them, and re-layouts  3.15 us (2%)
    pallas_call x1, Pallas kernels, per_device(): pl.pallas_call(kernel, out_shape=jax.ShapeDtypeStruct((2 * ROWS, 256), F3...  126 us
    unnamed x2, local copies, waits for them, and re-layouts  3.15 us

profile of v1, /device:TPU:1, one launch (start us, length us, event | category | flops | bytes accessed | tf_op | source)
XLA Modules:
  0.0 129.0 jit_solution(2457913167144702860)
XLA Ops:
  0.0 1.3 copy.9.taps
  1.3 125.9 %shard_map.82 = f32[512,256]{1,0:T(8,128)} custom-call(bf16[512,256]{1,0:T(8,128)(2,1)} %res.1, f32[2,4096]{1,0:T(2,128)} %norm_gain.1, bf16[2,256,128]{2,1,0:T(8,128)(2,1)} %gate.1, bf16[2,256,128]{2,1,0:T(8,128)(2,1)} %filt.1, bf16[2,256,128]{2,1,0:T(8,128)(2,1)} %sig.1, f32[2,3,128]{2,1,0:T(4,128)} %copy.9.taps, bf16[2,128,256]{2,1,0:T(8,128)(2,1)} %outp.1, ...), custom_call_target="tpu_custom_call" | custom-call | tf_op jit(solution)/shard_map/pallas_call | solution.py:397
  127.2 1.9 %copy.11 = f32[512,256]{1,0:T(8,128)} copy(f32[512,256]{1,0:T(8,128)} %shard_map.82) | data formatting | bytes 1048576

commit v2 on v1

v2 whole, which is shorter than its diff:
```python
import jax
import jax.numpy as jnp
from jax import lax
from jax.experimental import pallas as pl
from jax.experimental.pallas import tpu as pltpu
from jax.sharding import PartitionSpec as P

D = 4096
TAPS = 3
LAYERS = 2
FLOOR = 1e-06

NZ = 8
SIDE = 4
ROWS = 256
PIECE = 512
COLS = 256
CH = 128
WIDE = 512

F32 = jnp.float32
BF16 = jnp.bfloat16
MESH = pl.DeviceIdType.MESH

GATHER = (((96, 80), (176, 80), (0, 48), (48, 48)), ((112, 80), (192, 64), (0, 64), (64, 48)))
REDUCE = (((112, 80), (192, 64), (0, 64), (64, 48)), ((128, 64), (192, 64), (0, 64), (64, 64)))
GROUPS = ((0, 1), (2, 3))


def span(units, group):
    lo = units[GROUPS[group][0]][0]
    return lo, sum(units[u][1] for u in GROUPS[group])


def aligned(index, size):
    return pl.ds(pl.multiple_of(index * size, size), size)


def has(way, far, unit):
    return not far or (unit % 2 == 0) == (way == 0)


def kernel(
    res, norm_gain, gate, filt, sig, taps, outp, final_gain, out,
    x_all, res_other, xg, w_all, w_out, acc, prod, mixed, sq, rs_out, rs_in, halo, tap_all, gain_in, gain_out,
    sums, st, fin_out, fin_in,
    loc, ag0_s, ag0_r, ag_s, ag_r, w_s, w_r, d_s, d_r, rs_s, rs_r, h_s, h_r, s_s, s_r, m_s, m_r,
):
    s = lax.axis_index("sp")
    t = lax.axis_index("tp")
    z, c = t // 2, t % 2
    y, x = s // SIDE, s % SIDE
    other = 1 - c
    partner = (s, 2 * z + other)

    def at_z(k, core=None):
        return (s, ((z + k + NZ) % NZ) * 2 + (c if core is None else core))

    def at_x(k):
        return (y * SIDE + (x + k + SIDE) % SIDE, t)

    def at_y(k):
        return (((y + k + SIDE) % SIDE) * SIDE + x, t)

    halo_next = ((s + c) % 16, 2 * z + other)
    halo_far = ((s + 2 * c + 15) % 16, 2 * z + other)

    def rdma(src, dst, send, recv, device):
        return pltpu.make_async_remote_copy(
            src_ref=src, dst_ref=dst, send_sem=send, recv_sem=recv, device_id=device, device_id_type=MESH
        )

    pending = []

    def start(copy):
        copy.start()
        pending.append(copy)

    barrier = pltpu.get_barrier_semaphore()
    peers = [at_z(1), at_z(-1), at_z(1, other), at_z(-1, other), at_x(1), at_x(-1), at_y(1), at_y(-1), partner]
    for peer in peers:
        pl.semaphore_signal(barrier, inc=1, device_id=peer, device_id_type=MESH)

    own_cols = aligned(c, COLS)
    other_cols = aligned(other, COLS)
    own_rows = aligned(c, ROWS)
    other_rows = aligned(other, ROWS)
    own_wide = aligned(c, WIDE)

    local = []

    def place(src, dst):
        copy = pltpu.make_async_copy(src, dst, loc.at[len(local)])
        copy.start()
        local.append(copy)

    place(res.at[own_rows, :], x_all.at[0, z, :, own_cols])
    place(res.at[other_rows, :], res_other)
    for l in range(LAYERS):
        for part, ref in enumerate((gate, filt, sig)):
            first = pl.multiple_of(c * 3 * CH + (part + 1) * CH, CH)
            place(ref.at[l], w_all.at[l, aligned(s, 256), pl.ds(first, CH)])
        for h in range(2):
            place(
                outp.at[l, :, pl.ds(h * CH, CH)],
                w_all.at[l, aligned(2 * s + h, CH), aligned(c * 7, CH)],
            )
    place(norm_gain, gain_in)
    place(taps, tap_all.at[c])
    place(final_gain, gain_out)

    with jax.named_scope("barrier"):
        pl.semaphore_wait(barrier, len(peers))
    with jax.named_scope("local"):
        for copy in local:
            copy.wait()

    def piece(l, axis, along, across, lo, size):
        if axis == 0:
            yy, xx = y + across, x + along
        else:
            yy, xx = y + along, x + across
        index = ((yy + SIDE) % SIDE) * SIDE + (xx + SIDE) % SIDE
        return w_all.at[l, pl.ds(pl.multiple_of(index * 256 + lo, 64), size), own_wide]

    def w_copy(l, group, half, axis, across, sign, fwd, sending):
        step = sign if fwd else 0
        along = -step if sending else -step - sign
        lo, size = half * 128, 128
        if fwd:
            lo, size = lo + (0 if sign == 1 else 64), 64
        slot = group * 4 + (2 if fwd else 0) + (0 if sign == 1 else 1)
        ref = piece(l, axis, along, across, lo, size)
        device = at_x(sign) if axis == 0 else at_y(sign)
        return rdma(ref, ref, w_s.at[l, slot], w_r.at[l, slot], device)

    groups = {("a", 1): (0, 0, 0, 0), ("b", 1): (5, 1, 1, 0)}
    for i, p in enumerate((0, -1, 1, 2)):
        groups["a", 2, p] = (1 + i, 0, 1, p)
        groups["b", 2, p] = (6 + i, 1, 0, p)

    def w_send(l, *name):
        group, half, axis, across = groups[name]
        for sign in (1, -1):
            start(w_copy(l, group, half, axis, across, sign, False, True))

    def w_forward(l, *name):
        group, half, axis, across = groups[name]
        for sign in (1, -1):
            w_copy(l, group, half, axis, across, sign, False, False).wait_recv()
            start(w_copy(l, group, half, axis, across, sign, True, True))

    def w_finish(l, *name):
        group, half, axis, across = groups[name]
        for sign in (1, -1):
            w_copy(l, group, half, axis, across, sign, True, False).wait_recv()

    def w_row(l, k, core):
        return w_all.at[l, aligned((y + k + SIDE) % SIDE, 1024), aligned(core, WIDE)]

    def w_hand(l, k):
        slot = (k + SIDE) % SIDE
        start(rdma(w_row(l, k, c), w_row(l, k, c), d_s.at[l, slot], d_r.at[l, slot], partner))

    def w_taken(l, k):
        slot = (k + SIDE) % SIDE
        with jax.named_scope(f"taken#l={l}#k={k}"):
            rdma(w_row(l, k, other), w_row(l, k, other), d_s.at[l, slot], d_r.at[l, slot], partner).wait_recv()

    def w_stage(l, stage):
        with jax.named_scope(f"w#l={l}#s={stage}"):
            w_stage_body(l, stage)

    def w_stage_body(l, stage):
        if stage == 0:
            w_send(l, "a", 1)
            w_send(l, "b", 1)
            w_send(l, "b", 2, 0)
            w_send(l, "a", 2, 0)
        elif stage == 1:
            w_forward(l, "a", 1)
            w_forward(l, "b", 1)
            for p in (-1, 1):
                w_send(l, "a", 2, p)
                w_send(l, "b", 2, p)
        elif stage == 2:
            w_forward(l, "b", 2, 0)
            w_forward(l, "a", 2, 0)
            w_finish(l, "a", 1)
            w_send(l, "a", 2, 2)
            w_finish(l, "b", 1)
            w_send(l, "b", 2, 2)
        elif stage == 3:
            for p in (-1, 1):
                w_forward(l, "a", 2, p)
                w_forward(l, "b", 2, p)
            w_finish(l, "a", 2, 0)
            w_finish(l, "b", 2, 0)
            w_hand(l, 0)
        elif stage == 4:
            w_forward(l, "a", 2, 2)
            w_forward(l, "b", 2, 2)
            for p in (-1, 1):
                w_finish(l, "a", 2, p)
                w_finish(l, "b", 2, p)
            w_hand(l, -1)
            w_hand(l, 1)
        else:
            w_finish(l, "a", 2, 2)
            w_finish(l, "b", 2, 2)
            w_hand(l, 2)

    def build_w_out(l, k):
        first = ((y + k + SIDE) % SIDE) * 8

        def body(i, carry):
            for core in range(2):
                w_out[core * CH : (core + 1) * CH, aligned(first + i, CH)] = w_all[
                    l, aligned(first + i, CH), core * 7 * CH : (core * 7 + 1) * CH
                ]
            return carry

        lax.fori_loop(0, 8, body, 0)

    def chunk_at(k):
        return (z + k + NZ) % NZ

    def ag_copy(l, way, dist, unit, sending):
        sign = 1 - 2 * way
        lo, size = GATHER[l][unit]
        ref = x_all.at[l, chunk_at(-sign * (dist if sending else dist + 1)), pl.ds(lo, size), :]
        slot = dist * 4 + unit
        return rdma(ref, ref, ag_s.at[l, way, slot], ag_r.at[l, way, slot], at_z(sign))

    def first_copy(way, unit, crossing, sending):
        sign = 1 - 2 * way
        lo, size = GATHER[0][unit]
        cols = own_cols if sending or not crossing else other_cols
        dst = x_all.at[0, z if sending else chunk_at(-sign), pl.ds(lo, size), cols]
        src = res_other.at[pl.ds(lo, size), :] if crossing else x_all.at[0, z, pl.ds(lo, size), own_cols]
        slot = unit * 2 + (1 if crossing else 0)
        return rdma(src, dst, ag0_s.at[way, slot], ag0_r.at[way, slot], at_z(sign, other if crossing else c))

    def ag_first(l, unit):
        for way in range(2):
            if l == 0:
                start(first_copy(way, unit, False, True))
                start(first_copy(way, unit, True, True))
            else:
                start(ag_copy(l, way, 0, unit, True))

    def ag_step(l, dist, unit):
        with jax.named_scope(f"ag#l={l}#d={dist}#u={unit}"):
            for way in range(2):
                if not has(way, dist == 3, unit):
                    continue
                if l == 0 and dist == 0:
                    first_copy(way, unit, False, False).wait_recv()
                    first_copy(way, unit, True, False).wait_recv()
                else:
                    ag_copy(l, way, dist, unit, False).wait_recv()
                if dist < 3 and has(way, dist == 2, unit):
                    start(ag_copy(l, way, dist + 1, unit, True))

    def take(l, group, chunk):
        lo, size = span(GATHER[l], group)
        rows = pl.ds(lo, size)
        value = x_all[l, chunk, rows, :].astype(F32)
        square = value * value
        total = square[:, :128]
        for i in range(1, PIECE // 128):
            total = total + square[:, i * 128 : (i + 1) * 128]
        sq[rows, :] += total
        xg[chunk, rows, :] = (value * gain_in[l : l + 1, aligned(chunk, PIECE)]).astype(BF16)

    def arrived_at(dist):
        return (-dist - 1, dist + 1) if dist < 3 else (4,)

    def multiply(l, group, chunk):
        lo, size = span(GATHER[l], group)
        acc[lo : lo + size, :] += jnp.dot(
            xg[chunk, lo : lo + size, :],
            w_all[l, aligned(chunk, PIECE), CH : 7 * CH],
            preferred_element_type=F32,
        )

    def multiply_row(l, group, k):
        first = ((y + k + SIDE) % SIDE) * 2
        with jax.named_scope(f"mult#g={group}"):
            multiply(l, group, first)
            multiply(l, group, first + 1)

    def start_sums():
        sq[...] = jnp.zeros_like(sq)
        acc[...] = jnp.zeros_like(acc)

    def gates(l, group):
        lo, size = span(GATHER[l], group)
        rows = pl.ds(lo, size)
        mean = jnp.sum(sq[rows, :], axis=1, keepdims=True) / D
        scale = lax.rsqrt(mean + FLOOR)
        for core in range(2):
            base = core * 3 * CH
            value = (acc[rows, base + CH : base + 2 * CH] * scale) * (acc[rows, base + 2 * CH : base + 3 * CH] * scale)
            prod[pl.ds(8 + lo, size), core * CH : (core + 1) * CH] = value.astype(BF16).astype(F32)
            acc[rows, base : base + CH] = acc[rows, base : base + CH] * scale

    def mix(l, group):
        lo, size = span(REDUCE[l], group)
        rows = pl.ds(lo, size)
        for core in range(2):
            cols = pl.ds(core * CH, CH)
            filtered = jnp.zeros((size, CH), F32)
            for k in range(TAPS):
                tap = tap_all[core, k, l : l + 1, :]
                filtered = filtered + tap * prod[pl.ds(8 + lo - (TAPS - 1) + k, size), cols]
            gated = acc[rows, core * 3 * CH : core * 3 * CH + CH]
            mixed[rows, cols] = (gated * filtered).astype(BF16)

    def halo_copy(l):
        return rdma(halo.at[l, 0], halo.at[l, 1], h_s.at[l], h_r.at[l], halo_next)

    def give_halo(l):
        halo[l, 0] = prod[ROWS:, :]
        start(halo_copy(l))

    def take_halo(l):
        with jax.named_scope("halo"):
            halo_copy(l).wait_recv()
        first = jnp.logical_and(s == 0, c == 0)
        prod[:8, :] = jnp.where(first, 0.0, halo[l, 1])

    def rs_copy(l, way, k, unit):
        lo, size = REDUCE[l][unit]
        rows = pl.ds(lo, size)
        slot = (k - 1) * 4 + unit
        return rdma(
            rs_out.at[l, way, k - 1, rows, :], rs_in.at[l, way, k - 1, rows, :],
            rs_s.at[l, way, slot], rs_r.at[l, way, slot], at_z(1 - 2 * way),
        )

    def partial(l, unit, chunk):
        lo, size = REDUCE[l][unit]
        return jnp.dot(mixed[lo : lo + size, :], w_out[:, aligned(chunk, PIECE)], preferred_element_type=F32)

    def arrived(l, way, k, unit):
        rs_copy(l, way, k, unit).wait_recv()
        lo, size = REDUCE[l][unit]
        return rs_in[l, way, k - 1, lo : lo + size, :].astype(F32)

    def rs_step(l, i, group):
        for unit in GROUPS[group][::-1]:
            with jax.named_scope(f"rs#l={l}#i={i}#u={unit}"):
                lo, size = REDUCE[l][unit]
                for way in range(2):
                    k = 4 - i if has(way, True, unit) else 3 - i
                    if k < 1:
                        continue
                    value = partial(l, unit, chunk_at(k * (1 - 2 * way)))
                    if i > 0:
                        value = value + arrived(l, way, k + 1, unit)
                    rs_out[l, way, k - 1, lo : lo + size, :] = value.astype(BF16)
                    start(rs_copy(l, way, k, unit))

    def rs_last(l, unit):
        with jax.named_scope(f"last#l={l}#u={unit}"):
            lo, size = REDUCE[l][unit]
            value = partial(l, unit, z)
            for way in range(2):
                value = value + arrived(l, way, 1, unit)
            return (x_all[l, z, lo : lo + size, :].astype(F32) + value).astype(BF16)

    ag_first(0, 0)
    ag_first(0, 1)
    w_stage(0, 0)
    start(rdma(res_other, x_all.at[0, z, :, own_cols], m_s.at[0], m_r.at[0], partner))
    start(rdma(tap_all.at[c], tap_all.at[c], m_s.at[1], m_r.at[1], partner))
    ag_first(0, 2)
    ag_first(0, 3)
    start_sums()
    own_block = rdma(res_other, x_all.at[0, z, :, other_cols], m_s.at[0], m_r.at[0], partner)
    own_block.wait_recv()
    take(0, 0, z)
    take(0, 1, z)

    ag_step(0, 0, 0)
    w_stage(0, 1)
    ag_step(0, 0, 1)
    for k in arrived_at(0):
        take(0, 0, chunk_at(k))
    w_stage(0, 2)
    ag_step(0, 0, 2)
    ag_step(0, 0, 3)
    for k in arrived_at(0):
        take(0, 1, chunk_at(k))
    ag_step(0, 1, 0)
    ag_step(0, 1, 1)
    w_stage(0, 3)
    for k in arrived_at(1):
        take(0, 0, chunk_at(k))
    ag_step(0, 1, 2)
    ag_step(0, 1, 3)
    for k in arrived_at(1):
        take(0, 1, chunk_at(k))
    ag_step(0, 2, 0)
    ag_step(0, 2, 1)
    for k in arrived_at(2):
        take(0, 0, chunk_at(k))
    w_stage(0, 4)
    ag_step(0, 2, 2)
    ag_step(0, 2, 3)
    for k in arrived_at(2):
        take(0, 1, chunk_at(k))
    ag_step(0, 3, 0)
    ag_step(0, 3, 1)
    take(0, 0, chunk_at(4))
    w_taken(0, 0)
    multiply_row(0, 0, 0)
    w_stage(0, 5)
    w_stage(1, 0)
    for k in (-1, 1):
        w_taken(0, k)
        multiply_row(0, 0, k)
    ag_step(0, 3, 2)
    ag_step(0, 3, 3)
    take(0, 1, chunk_at(4))
    for k in (0, -1, 1):
        build_w_out(0, k)
    w_taken(0, 2)
    multiply_row(0, 0, 2)
    build_w_out(0, 2)
    rdma(tap_all.at[other], tap_all.at[other], m_s.at[1], m_r.at[1], partner).wait_recv()

    gates(0, 0)
    give_halo(0)
    mix(0, 0)
    rs_step(0, 0, 0)
    for k in (0, -1, 1, 2):
        multiply_row(0, 1, k)
    gates(0, 1)
    take_halo(0)
    mix(0, 1)
    rs_step(0, 0, 1)
    for i in (1, 2, 3):
        w_stage(1, i)
        rs_step(0, i, 0)
        rs_step(0, i, 1)
    start_sums()
    for group in range(2):
        for unit in GROUPS[group]:
            lo, size = REDUCE[0][unit]
            x_all[1, z, lo : lo + size, :] = rs_last(0, unit)
            ag_first(1, unit)
    w_stage(1, 4)
    w_stage(1, 5)
    for group in range(2):
        take(1, group, z)
    for k in (0, -1, 1, 2):
        w_taken(1, k)
        build_w_out(1, k)
    for group in range(2):
        multiply(1, group, z)
    for dist in range(3):
        for group in range(2):
            for unit in GROUPS[group]:
                ag_step(1, dist, unit)
            for k in arrived_at(dist):
                take(1, group, chunk_at(k))
                multiply(1, group, chunk_at(k))
    for group in range(2):
        for unit in GROUPS[group]:
            ag_step(1, 3, unit)
        take(1, group, chunk_at(4))
        multiply(1, group, chunk_at(4))
        gates(1, group)
        if group == 0:
            give_halo(1)
        else:
            take_halo(1)
        mix(1, group)
        rs_step(1, 0, group)
    for i in (1, 2, 3):
        rs_step(1, i, 0)
        rs_step(1, i, 1)

    def fin_copy(group):
        rows = pl.ds(*span(REDUCE[1], group))
        return rdma(fin_out.at[rows, :], fin_in.at[rows, :], m_s.at[2 + group], m_r.at[2 + group], partner)

    def sums_copy(group, k, crossing, sending):
        cols = pl.ds(*span(REDUCE[1], group))
        core = other if crossing and not sending else c
        ref = sums.at[core, z if sending else chunk_at(-k), :, cols]
        slot = 2 * k + (1 if crossing else 0)
        return rdma(ref, ref, s_s.at[group, slot], s_r.at[group, slot], at_z(k, other if crossing else c))

    routes = [(4, 0), (4, 1), (3, 0), (3, 1), (5, 0), (5, 1), (2, 0), (2, 1), (6, 0), (6, 1)]
    routes += [(1, 0), (1, 1), (7, 0), (7, 1), (0, 1)]
    for group in range(2):
        for unit in GROUPS[group]:
            lo, size = REDUCE[1][unit]
            st[lo : lo + size, :] = rs_last(1, unit).astype(F32)
        lo, size = span(REDUCE[1], group)
        rows = pl.ds(lo, size)
        value = st[rows, :]
        square = jnp.sum(value * value, axis=1, keepdims=True)
        sums[c, z, :, lo : lo + size] = jnp.broadcast_to(square, (size, 128)).T[:8, :]
        for k, crossing in routes:
            start(sums_copy(group, k, crossing, True))
        fin_out[rows, :] = st[rows, other_cols].astype(BF16)
        start(fin_copy(group))

    def scale_of(core):
        total = jnp.sum(sums[core, :, 0, :], axis=0, keepdims=True)
        return lax.rsqrt(jnp.broadcast_to(total, (128, ROWS)).T[:, :1] / D + FLOOR)

    with jax.named_scope("sums"):
        for group in range(2):
            fin_copy(group).wait_recv()
            for k, crossing in routes[::-1]:
                sums_copy(group, k, crossing, False).wait_recv()
    out[own_rows, :] = st[:, own_cols] * scale_of(c) * gain_out[...]
    out[other_rows, :] = fin_in[...].astype(F32) * scale_of(other) * gain_out[...]
    with jax.named_scope("sends"):
        for copy in pending:
            copy.wait_send()


def per_device(residual_in, norm_gain, gate_proj, filter_proj, signal_proj, conv_taps, out_proj, final_gain):
    dma = pltpu.SemaphoreType.DMA
    return pl.pallas_call(
        kernel,
        out_shape=jax.ShapeDtypeStruct((2 * ROWS, COLS), F32),
        in_specs=[pl.BlockSpec(memory_space=pltpu.HBM)] * 8,
        out_specs=pl.BlockSpec(memory_space=pltpu.VMEM),
        scratch_shapes=[
            pltpu.VMEM((LAYERS, NZ, ROWS, PIECE), BF16),
            pltpu.VMEM((ROWS, COLS), BF16),
            pltpu.VMEM((NZ, ROWS, PIECE), BF16),
            pltpu.VMEM((LAYERS, D, 2 * WIDE), BF16),
            pltpu.VMEM((2 * CH, D), BF16),
            pltpu.VMEM((ROWS, 6 * CH), F32),
            pltpu.VMEM((8 + ROWS, 2 * CH), F32),
            pltpu.VMEM((ROWS, 2 * CH), BF16),
            pltpu.VMEM((ROWS, 128), F32),
            pltpu.VMEM((LAYERS, 2, 4, ROWS, PIECE), BF16),
            pltpu.VMEM((LAYERS, 2, 4, ROWS, PIECE), BF16),
            pltpu.VMEM((LAYERS, 2, 8, 2 * CH), F32),
            pltpu.VMEM((2, TAPS, LAYERS, CH), F32),
            pltpu.VMEM((LAYERS, D), F32),
            pltpu.VMEM((1, COLS), F32),
            pltpu.VMEM((2, NZ, 8, ROWS), F32),
            pltpu.VMEM((ROWS, PIECE), F32),
            pltpu.VMEM((ROWS, COLS), BF16),
            pltpu.VMEM((ROWS, COLS), BF16),
            dma((16,)),
            dma((2, 8)), dma((2, 8)),
            dma((LAYERS, 2, 16)), dma((LAYERS, 2, 16)),
            dma((LAYERS, 40)), dma((LAYERS, 40)),
            dma((LAYERS, SIDE)), dma((LAYERS, SIDE)),
            dma((LAYERS, 2, 16)), dma((LAYERS, 2, 16)),
            dma((LAYERS,)), dma((LAYERS,)),
            dma((2, 16)), dma((2, 16)),
            dma((4,)), dma((4,)),
        ],
        compiler_params=pltpu.CompilerParams(
            collective_id=0, has_side_effects=True, vmem_limit_bytes=58 * 1024 * 1024
        ),
    )(
        residual_in, norm_gain, gate_proj, filter_proj, signal_proj, jnp.transpose(conv_taps, (1, 0, 2)), out_proj,
        final_gain.reshape(1, -1),
    )


def solution(mesh):
    return jax.shard_map(
        per_device,
        mesh=mesh,
        in_specs=(
            P("sp", "tp"),
            P(),
            P(None, "sp", "tp"),
            P(None, "sp", "tp"),
            P(None, "sp", "tp"),
            P(None, None, "tp"),
            P(None, "tp", "sp"),
            P("tp"),
        ),
        out_specs=P("sp", "tp"),
        check_vma=False,
    )
```

time: 129 us -> 122 us (0.946)
  Pallas kernels: 126 us -> 120 us
    pallas_call x1, Pallas kernels: 126 us -> 120 us  [per_device(): pl.pallas_call(kernel, out_shape=jax.ShapeDtypeStruct((2 * ROWS, COLS), F...]
    unnamed x2 -> x1, local copies, waits for them, and re-layouts: 3.15 us -> 1.87 us
where the time goes in v2:
time: 122 us; the launch traced here: 121 us
  Pallas kernels  120 us (98%)
  local copies, waits for them, and re-layouts  1.87 us (2%)
    pallas_call x1, Pallas kernels, per_device(): pl.pallas_call(kernel, out_shape=jax.ShapeDtypeStruct((2 * ROWS, COLS), F...  120 us

profile of v2, /device:TPU:1, one launch (start us, length us, event | category | flops | bytes accessed | tf_op | source)
XLA Modules:
  0.0 121.4 jit_solution(17323309958854516900)
XLA Ops:
  0.0 119.5 %shard_map.82 = f32[512,256]{1,0:T(8,128)} custom-call(bf16[512,256]{1,0:T(8,128)(2,1)} %res.1, f32[2,4096]{1,0:T(2,128)} %norm_gain.1, bf16[2,256,128]{2,1,0:T(8,128)(2,1)} %gate.1, bf16[2,256,128]{2,1,0:T(8,128)(2,1)} %filt.1, bf16[2,256,128]{2,1,0:T(8,128)(2,1)} %sig.1, f32[3,2,128]{2,1,0:T(2,128)} %bitcast.2, bf16[2,128,256]{2,1,0:T(8,128)(2,1)} %outp.1, ...), custom_call_target="tpu_custom_call" | custom-call | tf_op jit(solution)/shard_map/pallas_call | solution.py:531
  119.5 1.9 %copy.10 = f32[512,256]{1,0:T(8,128)} copy(f32[512,256]{1,0:T(8,128)} %shard_map.82) | data formatting | bytes 1048576

commit v3 on v2

v3 whole, which is shorter than its diff:
```python
import jax
import jax.numpy as jnp
from jax import lax
from jax.experimental import pallas as pl
from jax.experimental.pallas import tpu as pltpu
from jax.sharding import PartitionSpec as P

D = 4096
TAPS = 3
LAYERS = 2
FLOOR = 1e-06

NZ = 8
SIDE = 4
ROWS = 256
PIECE = 512
COLS = 256
CH = 128
WIDE = 512

F32 = jnp.float32
BF16 = jnp.bfloat16
MESH = pl.DeviceIdType.MESH

GATHER = (((96, 80), (176, 80), (0, 48), (48, 48)), ((112, 80), (192, 64), (0, 64), (64, 48)))
REDUCE = (((112, 80), (192, 64), (0, 64), (64, 48)), ((128, 64), (192, 64), (0, 64), (64, 64)))
GROUPS = ((0, 1), (2, 3))


SENT_ROWS = (7680, 8192, 3584, 3584, 392)


def span(units, group):
    lo = units[GROUPS[group][0]][0]
    return lo, sum(units[u][1] for u in GROUPS[group])


def aligned(index, size):
    return pl.ds(pl.multiple_of(index * size, size), size)


def has(way, far, unit):
    return not far or (unit % 2 == 0) == (way == 0)


def kernel(
    res, norm_gain, gate, filt, sig, taps, outp, final_gain, out,
    x_all, res_other, xg, w_all, w_out, acc, prod, mixed, sq, rs_out, rs_in, halo, tap_all, gain_in, gain_out,
    sums, st, fin_out, fin_in,
    loc, sent, ag0_r, ag_r, w_r, d_r, rs_r, h_r, s_r, m_r,
):
    s = lax.axis_index("sp")
    t = lax.axis_index("tp")
    z, c = t // 2, t % 2
    y, x = s // SIDE, s % SIDE
    other = 1 - c
    partner = (s, 2 * z + other)

    def at_z(k, core=None):
        return (s, ((z + k + NZ) % NZ) * 2 + (c if core is None else core))

    def at_x(k):
        return (y * SIDE + (x + k + SIDE) % SIDE, t)

    def at_y(k):
        return (((y + k + SIDE) % SIDE) * SIDE + x, t)

    halo_next = ((s + c) % 16, 2 * z + other)
    halo_far = ((s + 2 * c + 15) % 16, 2 * z + other)

    def rdma(src, dst, send, recv, device):
        return pltpu.make_async_remote_copy(
            src_ref=src, dst_ref=dst, send_sem=send, recv_sem=recv, device_id=device, device_id_type=MESH
        )

    def start(copy):
        copy.start()

    barrier = pltpu.get_barrier_semaphore()
    peers = [at_z(1), at_z(-1), at_z(1, other), at_z(-1, other), at_x(1), at_x(-1), at_y(1), at_y(-1), partner]
    for peer in peers:
        pl.semaphore_signal(barrier, inc=1, device_id=peer, device_id_type=MESH)

    own_cols = aligned(c, COLS)
    other_cols = aligned(other, COLS)
    own_rows = aligned(c, ROWS)
    other_rows = aligned(other, ROWS)

    local = []

    def place(src, dst):
        copy = pltpu.make_async_copy(src, dst, loc.at[0])
        copy.start()
        local.append(copy)

    place(res.at[own_rows, :], x_all.at[0, z, :, own_cols])
    place(res.at[other_rows, :], res_other)
    for l in range(LAYERS):
        for part, ref in enumerate((gate, filt, sig)):
            first = pl.multiple_of(c * 3 * CH + (part + 1) * CH, CH)
            place(ref.at[l], w_all.at[l, aligned(s, 256), pl.ds(first, CH)])
        for h in range(2):
            place(
                outp.at[l, :, pl.ds(h * CH, CH)],
                w_all.at[l, aligned(2 * s + h, CH), aligned(c * 7, CH)],
            )
    place(norm_gain, gain_in)
    place(taps, tap_all.at[c])
    place(final_gain, gain_out)

    with jax.named_scope("barrier"):
        pl.semaphore_wait(barrier, len(peers))
    with jax.named_scope("local"):
        for copy in local:
            copy.wait()

    def lanes(what, core):
        if what == "proj":
            return pl.ds(pl.multiple_of(core * 3 * CH + CH, CH), 3 * CH)
        if what == "out":
            return aligned(core * 7, CH)
        return aligned(core, WIDE)

    carriers = ((0, "proj", 0, 64), (0, "proj", 64, 64), (0, "out", 0, 128), (1, "both", 0, 128))

    def w_copy(carrier, group, half, axis, across, sign, fwd, sending):
        l, what, first, size = carriers[carrier]
        step = sign if fwd else 0
        along = -step if sending else -step - sign
        lo = half * 128 + first
        if fwd:
            size = size // 2
            lo += 0 if sign == 1 else size
        if axis == 0:
            yy, xx = y + across, x + along
        else:
            yy, xx = y + along, x + across
        index = ((yy + SIDE) % SIDE) * SIDE + (xx + SIDE) % SIDE
        ref = w_all.at[l, pl.ds(pl.multiple_of(index * 256 + lo, 32), size), lanes(what, c)]
        slot = group * 4 + (2 if fwd else 0) + (0 if sign == 1 else 1)
        device = at_x(sign) if axis == 0 else at_y(sign)
        return rdma(ref, ref, sent.at[0], w_r.at[carrier % 3, slot], device)

    groups = {("a", 1): (0, 0, 0, 0), ("b", 1): (5, 1, 1, 0)}
    for i, p in enumerate((0, -1, 1, 2)):
        groups["a", 2, p] = (1 + i, 0, 1, p)
        groups["b", 2, p] = (6 + i, 1, 0, p)

    def w_send(carrier, *name):
        group, half, axis, across = groups[name]
        for sign in (1, -1):
            start(w_copy(carrier, group, half, axis, across, sign, False, True))

    def w_forward(carrier, *name):
        group, half, axis, across = groups[name]
        for sign in (1, -1):
            w_copy(carrier, group, half, axis, across, sign, False, False).wait_recv()
            start(w_copy(carrier, group, half, axis, across, sign, True, True))

    def w_finish(carrier, *name):
        group, half, axis, across = groups[name]
        for sign in (1, -1):
            w_copy(carrier, group, half, axis, across, sign, True, False).wait_recv()

    parcels = ((0, "proj"), (0, "out"), (1, "both"))

    def w_parcel(parcel, k, core):
        l, what = parcels[parcel]
        ref = w_all.at[l, aligned((y + k + SIDE) % SIDE, 1024), lanes(what, core)]
        slot = (k + SIDE) % SIDE
        return rdma(ref, ref, sent.at[1], d_r.at[parcel, slot], partner)

    def w_hand(parcel, *ks):
        for k in ks:
            start(w_parcel(parcel, k, c))

    def w_taken(parcel, k):
        with jax.named_scope(f"taken#p={parcel}#k={k}"):
            w_parcel(parcel, k, other).wait_recv()

    def w_stage(carrier, stage):
        with jax.named_scope(f"w#t={carrier}#s={stage}"):
            w_stage_body(carrier, stage)

    def w_stage_body(t, stage):
        if stage == 0:
            w_send(t, "a", 1)
            w_send(t, "b", 1)
            w_send(t, "b", 2, 0)
            w_send(t, "a", 2, 0)
        elif stage == 1:
            w_forward(t, "a", 1)
            w_forward(t, "b", 1)
            for p in (-1, 1):
                w_send(t, "a", 2, p)
                w_send(t, "b", 2, p)
        elif stage == 2:
            w_forward(t, "b", 2, 0)
            w_forward(t, "a", 2, 0)
            w_finish(t, "a", 1)
            w_send(t, "a", 2, 2)
            w_finish(t, "b", 1)
            w_send(t, "b", 2, 2)
        elif stage == 3:
            for p in (-1, 1):
                w_forward(t, "a", 2, p)
                w_forward(t, "b", 2, p)
            w_finish(t, "a", 2, 0)
            w_finish(t, "b", 2, 0)
        elif stage == 4:
            w_forward(t, "a", 2, 2)
            w_forward(t, "b", 2, 2)
            for p in (-1, 1):
                w_finish(t, "a", 2, p)
                w_finish(t, "b", 2, p)
        else:
            w_finish(t, "a", 2, 2)
            w_finish(t, "b", 2, 2)

    def build_w_out(l, k):
        first = ((y + k + SIDE) % SIDE) * 8

        def body(i, carry):
            for core in range(2):
                w_out[core * CH : (core + 1) * CH, aligned(first + i, CH)] = w_all[
                    l, aligned(first + i, CH), core * 7 * CH : (core * 7 + 1) * CH
                ]
            return carry

        lax.fori_loop(0, 8, body, 0)

    def chunk_at(k):
        return (z + k + NZ) % NZ

    def ag_copy(l, way, dist, unit, sending):
        sign = 1 - 2 * way
        lo, size = GATHER[l][unit]
        ref = x_all.at[l, chunk_at(-sign * (dist if sending else dist + 1)), pl.ds(lo, size), :]
        slot = dist * 4 + unit
        return rdma(ref, ref, sent.at[2], ag_r.at[way, slot], at_z(sign))

    def first_copy(way, unit, crossing, sending):
        sign = 1 - 2 * way
        lo, size = GATHER[0][unit]
        cols = own_cols if sending or not crossing else other_cols
        dst = x_all.at[0, z if sending else chunk_at(-sign), pl.ds(lo, size), cols]
        src = res_other.at[pl.ds(lo, size), :] if crossing else x_all.at[0, z, pl.ds(lo, size), own_cols]
        slot = unit * 2 + (1 if crossing else 0)
        return rdma(src, dst, sent.at[2], ag0_r.at[way, slot], at_z(sign, other if crossing else c))

    def ag_first(l, unit):
        for way in range(2):
            if l == 0:
                start(first_copy(way, unit, False, True))
                start(first_copy(way, unit, True, True))
            else:
                start(ag_copy(l, way, 0, unit, True))

    def ag_step(l, dist, unit):
        with jax.named_scope(f"ag#l={l}#d={dist}#u={unit}"):
            for way in range(2):
                if not has(way, dist == 3, unit):
                    continue
                if l == 0 and dist == 0:
                    first_copy(way, unit, False, False).wait_recv()
                    first_copy(way, unit, True, False).wait_recv()
                else:
                    ag_copy(l, way, dist, unit, False).wait_recv()
                if dist < 3 and has(way, dist == 2, unit):
                    start(ag_copy(l, way, dist + 1, unit, True))

    def take(l, group, chunk):
        lo, size = span(GATHER[l], group)
        rows = pl.ds(lo, size)
        value = x_all[l, chunk, rows, :].astype(F32)
        square = value * value
        total = square[:, :128]
        for i in range(1, PIECE // 128):
            total = total + square[:, i * 128 : (i + 1) * 128]
        sq[rows, :] += total
        xg[chunk, rows, :] = (value * gain_in[l : l + 1, aligned(chunk, PIECE)]).astype(BF16)

    def arrived_at(dist):
        return (-dist - 1, dist + 1) if dist < 3 else (4,)

    def multiply(l, group, chunk):
        lo, size = span(GATHER[l], group)
        acc[lo : lo + size, :] += jnp.dot(
            xg[chunk, lo : lo + size, :],
            w_all[l, aligned(chunk, PIECE), CH : 7 * CH],
            preferred_element_type=F32,
        )

    def multiply_row(l, group, k):
        first = ((y + k + SIDE) % SIDE) * 2
        with jax.named_scope(f"mult#g={group}"):
            multiply(l, group, first)
            multiply(l, group, first + 1)

    def start_sums():
        sq[...] = jnp.zeros_like(sq)
        acc[...] = jnp.zeros_like(acc)

    def gates(l, group):
        lo, size = span(GATHER[l], group)
        rows = pl.ds(lo, size)
        mean = jnp.sum(sq[rows, :], axis=1, keepdims=True) / D
        scale = lax.rsqrt(mean + FLOOR)
        for core in range(2):
            base = core * 3 * CH
            value = (acc[rows, base + CH : base + 2 * CH] * scale) * (acc[rows, base + 2 * CH : base + 3 * CH] * scale)
            prod[pl.ds(8 + lo, size), core * CH : (core + 1) * CH] = value.astype(BF16).astype(F32)
            acc[rows, base : base + CH] = acc[rows, base : base + CH] * scale

    def mix(l, unit):
        lo, size = REDUCE[l][unit]
        rows = pl.ds(lo, size)
        for core in range(2):
            cols = pl.ds(core * CH, CH)
            filtered = jnp.zeros((size, CH), F32)
            for k in range(TAPS):
                tap = tap_all[core, k, l : l + 1, :]
                filtered = filtered + tap * prod[pl.ds(8 + lo - (TAPS - 1) + k, size), cols]
            gated = acc[rows, core * 3 * CH : core * 3 * CH + CH]
            mixed[rows, cols] = (gated * filtered).astype(BF16)

    def halo_copy(l):
        return rdma(halo.at[l, 0], halo.at[l, 1], sent.at[4], h_r.at[l], halo_next)

    def give_halo(l):
        halo[l, 0] = prod[ROWS:, :]
        start(halo_copy(l))

    def take_halo(l):
        with jax.named_scope("halo"):
            halo_copy(l).wait_recv()
        first = jnp.logical_and(s == 0, c == 0)
        prod[:8, :] = jnp.where(first, 0.0, halo[l, 1])

    def rs_copy(l, way, k, unit):
        lo, size = REDUCE[l][unit]
        rows = pl.ds(lo, size)
        slot = (k - 1) * 4 + unit
        return rdma(
            rs_out.at[l, way, k - 1, rows, :], rs_in.at[l, way, k - 1, rows, :],
            sent.at[3], rs_r.at[way, slot], at_z(1 - 2 * way),
        )

    def partial(l, unit, chunk):
        lo, size = REDUCE[l][unit]
        return jnp.dot(mixed[lo : lo + size, :], w_out[:, aligned(chunk, PIECE)], preferred_element_type=F32)

    def arrived(l, way, k, unit):
        rs_copy(l, way, k, unit).wait_recv()
        lo, size = REDUCE[l][unit]
        return rs_in[l, way, k - 1, lo : lo + size, :].astype(F32)

    def rs_step(l, i, unit):
        with jax.named_scope(f"rs#l={l}#i={i}#u={unit}"):
            lo, size = REDUCE[l][unit]
            for way in range(2):
                k = 4 - i if has(way, True, unit) else 3 - i
                if k < 1:
                    continue
                value = partial(l, unit, chunk_at(k * (1 - 2 * way)))
                if i > 0:
                    value = value + arrived(l, way, k + 1, unit)
                rs_out[l, way, k - 1, lo : lo + size, :] = value.astype(BF16)
                start(rs_copy(l, way, k, unit))

    def rs_last(l, unit):
        with jax.named_scope(f"last#l={l}#u={unit}"):
            lo, size = REDUCE[l][unit]
            value = partial(l, unit, z)
            for way in range(2):
                value = value + arrived(l, way, 1, unit)
            return (x_all[l, z, lo : lo + size, :].astype(F32) + value).astype(BF16)

    def take_step(l, group, dist):
        for k in arrived_at(dist):
            take(l, group, chunk_at(k))
            if l == 1:
                multiply(l, group, chunk_at(k))

    ag_first(0, 0)
    ag_first(0, 1)
    w_stage(0, 0)
    w_stage(1, 0)
    start(rdma(res_other, x_all.at[0, z, :, own_cols], sent.at[4], m_r.at[0], partner))
    start(rdma(tap_all.at[c], tap_all.at[c], sent.at[5], m_r.at[1], partner))
    ag_first(0, 2)
    ag_first(0, 3)
    start_sums()
    rdma(res_other, x_all.at[0, z, :, other_cols], sent.at[4], m_r.at[0], partner).wait_recv()
    take(0, 0, z)
    take(0, 1, z)

    w_stage(2, 0)
    w_stage(0, 1)
    ag_step(0, 0, 0)
    w_stage(1, 1)
    ag_step(0, 0, 1)
    take_step(0, 0, 0)
    ag_step(0, 0, 2)
    ag_step(0, 0, 3)
    take_step(0, 1, 0)
    w_stage(2, 1)
    w_stage(0, 2)
    ag_step(0, 1, 0)
    w_stage(1, 2)
    ag_step(0, 1, 1)
    take_step(0, 0, 1)
    ag_step(0, 1, 2)
    w_stage(0, 3)
    ag_step(0, 1, 3)
    take_step(0, 1, 1)
    w_stage(2, 2)
    w_stage(1, 3)
    w_hand(0, 0)
    ag_step(0, 2, 0)
    w_stage(0, 4)
    ag_step(0, 2, 1)
    take_step(0, 0, 2)
    w_stage(2, 3)
    w_stage(1, 4)
    w_hand(0, -1, 1)
    w_hand(1, 0)
    ag_step(0, 2, 2)
    ag_step(0, 2, 3)
    take_step(0, 1, 2)
    w_stage(0, 5)
    w_stage(2, 4)
    w_hand(1, -1, 1)
    ag_step(0, 3, 0)
    ag_step(0, 3, 1)
    take_step(0, 0, 3)
    w_stage(1, 5)
    w_hand(0, 2)
    w_taken(0, 0)
    multiply_row(0, 0, 0)
    w_taken(0, -1)
    multiply_row(0, 0, -1)
    w_stage(2, 5)
    w_hand(1, 2)
    w_stage(3, 0)
    for k in (1, 2):
        w_taken(0, k)
        multiply_row(0, 0, k)
    ag_step(0, 3, 2)
    ag_step(0, 3, 3)
    take_step(0, 1, 3)
    gates(0, 0)
    rdma(tap_all.at[other], tap_all.at[other], sent.at[4], m_r.at[1], partner).wait_recv()
    give_halo(0)
    mix(0, 1)
    mix(0, 0)
    for k in (0, -1, 1, 2):
        w_taken(1, k)
        build_w_out(0, k)

    rs_step(0, 0, 1)
    rs_step(0, 0, 0)
    for k in (0, -1, 1, 2):
        multiply_row(0, 1, k)
    gates(0, 1)
    mix(0, 3)
    rs_step(0, 0, 3)
    rs_step(0, 1, 1)
    take_halo(0)
    mix(0, 2)
    rs_step(0, 0, 2)
    start_sums()
    rs_step(0, 1, 0)
    rs_step(0, 1, 3)
    w_stage(3, 1)
    rs_step(0, 2, 1)
    rs_step(0, 1, 2)
    rs_step(0, 2, 0)
    rs_step(0, 2, 3)
    w_stage(3, 2)
    rs_step(0, 3, 1)
    rs_step(0, 2, 2)
    rs_step(0, 3, 0)
    rs_step(0, 3, 3)
    w_stage(3, 3)
    w_hand(2, 0)

    def next_stream(unit):
        lo, size = REDUCE[0][unit]
        x_all[1, z, lo : lo + size, :] = rs_last(0, unit)
        ag_first(1, unit)

    next_stream(1)
    rs_step(0, 3, 2)
    next_stream(0)
    take(1, 0, z)
    next_stream(3)
    next_stream(2)
    take(1, 1, z)

    ag_step(1, 0, 1)
    ag_step(1, 0, 0)
    w_stage(3, 4)
    w_hand(2, -1, 1)
    ag_step(1, 0, 3)
    ag_step(1, 0, 2)
    ag_step(1, 1, 1)
    ag_step(1, 1, 0)
    w_stage(3, 5)
    w_hand(2, 2)
    ag_step(1, 1, 3)
    ag_step(1, 1, 2)
    for k in (0, -1, 1, 2):
        w_taken(2, k)
        build_w_out(1, k)
    ag_step(1, 2, 1)
    for group in range(2):
        multiply(1, group, z)
        take_step(1, group, 0)
    ag_step(1, 2, 0)
    take_step(1, 0, 1)
    ag_step(1, 2, 3)
    take_step(1, 1, 1)
    ag_step(1, 2, 2)
    take_step(1, 0, 2)
    take_step(1, 1, 2)
    ag_step(1, 3, 1)
    ag_step(1, 3, 0)
    take_step(1, 0, 3)
    gates(1, 0)
    give_halo(1)
    mix(1, 1)
    mix(1, 0)
    rs_step(1, 0, 1)
    rs_step(1, 0, 0)
    ag_step(1, 3, 3)
    ag_step(1, 3, 2)
    take_step(1, 1, 3)
    gates(1, 1)
    mix(1, 3)
    rs_step(1, 0, 3)
    rs_step(1, 1, 1)
    take_halo(1)
    mix(1, 2)
    rs_step(1, 0, 2)
    rs_step(1, 1, 0)
    rs_step(1, 1, 3)
    rs_step(1, 2, 1)
    rs_step(1, 1, 2)
    rs_step(1, 2, 0)
    rs_step(1, 2, 3)
    rs_step(1, 3, 1)
    rs_step(1, 2, 2)
    rs_step(1, 3, 0)
    rs_step(1, 3, 3)
    rs_step(1, 3, 2)

    def fin_copy(group):
        rows = pl.ds(*span(REDUCE[1], group))
        return rdma(fin_out.at[rows, :], fin_in.at[rows, :], sent.at[4], m_r.at[2 + group], partner)

    def sums_copy(group, k, crossing):
        ref = sums.at[c, z, :, pl.ds(*span(REDUCE[1], group))]
        return rdma(ref, ref, sent.at[4], s_r.at[group, crossing], at_z(k, other if crossing else c))

    routes = [(4, 0), (4, 1), (3, 0), (3, 1), (5, 0), (5, 1), (2, 0), (2, 1), (6, 0), (6, 1)]
    routes += [(1, 0), (1, 1), (7, 0), (7, 1), (0, 1)]
    for group in range(2):
        for unit in GROUPS[group]:
            lo, size = REDUCE[1][unit]
            st[lo : lo + size, :] = rs_last(1, unit).astype(F32)
        lo, size = span(REDUCE[1], group)
        rows = pl.ds(lo, size)
        value = st[rows, :]
        square = jnp.sum(value * value, axis=1, keepdims=True)
        sums[c, z, :, lo : lo + size] = jnp.broadcast_to(square, (size, 128)).T[:8, :]
        for k, crossing in routes:
            start(sums_copy(group, k, crossing))
        fin_out[rows, :] = st[rows, other_cols].astype(BF16)
        start(fin_copy(group))

    def scale_of(core):
        total = jnp.sum(sums[core, :, 0, :], axis=0, keepdims=True)
        return lax.rsqrt(jnp.broadcast_to(total, (128, ROWS)).T[:, :1] / D + FLOOR)

    with jax.named_scope("sums"):
        for group in range(2):
            fin_copy(group).wait_recv()
            cols = pl.ds(*span(REDUCE[1], group))
            for crossing, ref in enumerate((sums.at[c, pl.ds(0, NZ - 1), :, cols], sums.at[other, :, :, cols])):
                rdma(ref, ref, sent.at[4], s_r.at[group, crossing], partner).wait_recv()
    out[own_rows, :] = st[:, own_cols] * scale_of(c) * gain_out[...]
    out[other_rows, :] = fin_in[...].astype(F32) * scale_of(other) * gain_out[...]
    with jax.named_scope("sends"):
        for kind, rows in enumerate(SENT_ROWS):
            ref = w_all.at[0, pl.ds(0, rows), pl.ds(0, WIDE)] if rows <= D else w_all.at[0, pl.ds(0, rows // 2), :]
            rdma(ref, ref, sent.at[kind], m_r.at[0], partner).wait_send()
        rdma(tap_all.at[c], tap_all.at[c], sent.at[5], m_r.at[1], partner).wait_send()


def per_device(residual_in, norm_gain, gate_proj, filter_proj, signal_proj, conv_taps, out_proj, final_gain):
    dma = pltpu.SemaphoreType.DMA
    return pl.pallas_call(
        kernel,
        out_shape=jax.ShapeDtypeStruct((2 * ROWS, COLS), F32),
        in_specs=[pl.BlockSpec(memory_space=pltpu.HBM)] * 8,
        out_specs=pl.BlockSpec(memory_space=pltpu.VMEM),
        scratch_shapes=[
            pltpu.VMEM((LAYERS, NZ, ROWS, PIECE), BF16),
            pltpu.VMEM((ROWS, COLS), BF16),
            pltpu.VMEM((NZ, ROWS, PIECE), BF16),
            pltpu.VMEM((LAYERS, D, 2 * WIDE), BF16),
            pltpu.VMEM((2 * CH, D), BF16),
            pltpu.VMEM((ROWS, 6 * CH), F32),
            pltpu.VMEM((8 + ROWS, 2 * CH), F32),
            pltpu.VMEM((ROWS, 2 * CH), BF16),
            pltpu.VMEM((ROWS, 128), F32),
            pltpu.VMEM((LAYERS, 2, 4, ROWS, PIECE), BF16),
            pltpu.VMEM((LAYERS, 2, 4, ROWS, PIECE), BF16),
            pltpu.VMEM((LAYERS, 2, 8, 2 * CH), F32),
            pltpu.VMEM((2, TAPS, LAYERS, CH), F32),
            pltpu.VMEM((LAYERS, D), F32),
            pltpu.VMEM((1, COLS), F32),
            pltpu.VMEM((2, NZ, 8, ROWS), F32),
            pltpu.VMEM((ROWS, PIECE), F32),
            pltpu.VMEM((ROWS, COLS), BF16),
            pltpu.VMEM((ROWS, COLS), BF16),
            dma((1,)),
            dma((6,)),
            dma((2, 8)),
            dma((2, 16)),
            dma((3, 40)),
            dma((3, SIDE)),
            dma((2, 16)),
            dma((LAYERS,)),
            dma((2, 2)),
            dma((4,)),
        ],
        compiler_params=pltpu.CompilerParams(
            collective_id=0, has_side_effects=True, vmem_limit_bytes=44 * 1024 * 1024
        ),
    )(
        *(
            pltpu.with_memory_space_constraint(a, pltpu.HBM)
            for a in (
                residual_in, norm_gain, gate_proj, filter_proj, signal_proj, jnp.transpose(conv_taps, (1, 0, 2)),
                out_proj, final_gain.reshape(1, -1),
            )
        )
    )


def solution(mesh):
    return jax.shard_map(
        per_device,
        mesh=mesh,
        in_specs=(
            P("sp", "tp"),
            P(),
            P(None, "sp", "tp"),
            P(None, "sp", "tp"),
            P(None, "sp", "tp"),
            P(None, None, "tp"),
            P(None, "tp", "sp"),
            P("tp"),
        ),
        out_specs=P("sp", "tp"),
        check_vma=False,
    )
```

time: 122 us -> 111 us (0.910)
  Pallas kernels: 120 us -> 111 us
    pallas_call x1, Pallas kernels: 120 us -> 111 us  [per_device(): pl.pallas_call(kernel, out_shape=jax.ShapeDtypeStruct((2 * ROWS, COLS), F...]
where the time goes in v3:
time: 111 us
  Pallas kernels  111 us (100%)
    pallas_call x1, Pallas kernels, per_device(): pl.pallas_call(kernel, out_shape=jax.ShapeDtypeStruct((2 * ROWS, COLS), F...  111 us

profile of v3, /device:TPU:1, one launch (start us, length us, event | category | flops | bytes accessed | tf_op | source)
XLA Modules:
  0.0 111.4 jit_solution(15827201890603994576)
XLA Ops:
  0.0 110.6 %shard_map.82 = f32[512,256]{1,0:T(8,128)S(1)} custom-call(bf16[512,256]{1,0:T(8,128)(2,1)} %res.1, f32[2,4096]{1,0:T(2,128)} %norm_gain.1, bf16[2,256,128]{2,1,0:T(8,128)(2,1)} %gate.1, bf16[2,256,128]{2,1,0:T(8,128)(2,1)} %filt.1, bf16[2,256,128]{2,1,0:T(8,128)(2,1)} %sig.1, f32[3,2,128]{2,1,0:T(2,128)} %bitcast.2, bf16[2,128,256]{2,1,0:T(8,128)(2,1)} %outp.1, ...), custom_call_target="tpu_custom_call" | custom-call | tf_op jit(solution)/shard_map/pallas_call | solution.py:603
  110.6 0.8 copy.10

commit v4 on v3

--- a/solution.py
+++ b/solution.py
@@ -22,10 +22,17 @@
 BF16 = jnp.bfloat16
 MESH = pl.DeviceIdType.MESH
 
-GATHER = (((96, 80), (176, 80), (0, 48), (48, 48)), ((112, 80), (192, 64), (0, 64), (64, 48)))
-REDUCE = (((112, 80), (192, 64), (0, 64), (64, 48)), ((128, 64), (192, 64), (0, 64), (64, 64)))
-GROUPS = ((0, 1), (2, 3))
-
+GATHER = (
+    ((96, 80), (176, 80), (0, 16), (16, 48), (64, 32)),
+    ((112, 80), (192, 64), (0, 16), (16, 48), (64, 48)),
+)
+REDUCE = (
+    ((112, 80), (192, 64), (0, 16), (16, 48), (64, 48)),
+    ((128, 64), (192, 64), (0, 16), (16, 64), (80, 48)),
+)
+GROUPS = ((0, 1), (2, 3, 4))
+UNITS = 5
+FAR = (0, 1, 1, 0, 1)
 
 SENT_ROWS = (7680, 8192, 3584, 3584, 392)
 
@@ -40,14 +47,14 @@
 
 
 def has(way, far, unit):
-    return not far or (unit % 2 == 0) == (way == 0)
+    return not far or FAR[unit] == way
 
 
 def kernel(
     res, norm_gain, gate, filt, sig, taps, outp, final_gain, out,
     x_all, res_other, xg, w_all, w_out, acc, prod, mixed, sq, rs_out, rs_in, halo, tap_all, gain_in, gain_out,
     sums, st, fin_out, fin_in,
-    loc, sent, ag0_r, ag_r, w_r, d_r, rs_r, h_r, s_r, m_r,
+    loc, sent, ag_r, w_r, d_r, rs_r, h_r, s_r, m_r,
 ):
     s = lax.axis_index("sp")
     t = lax.axis_index("tp")
@@ -65,8 +72,8 @@
     def at_y(k):
         return (((y + k + SIDE) % SIDE) * SIDE + x, t)
 
-    halo_next = ((s + c) % 16, 2 * z + other)
-    halo_far = ((s + 2 * c + 15) % 16, 2 * z + other)
+    half = 1 - c
+    halo_next = ((s + half) % 16, 2 * z + other)
 
     def rdma(src, dst, send, recv, device):
         return pltpu.make_async_remote_copy(
@@ -83,8 +90,8 @@
 
     own_cols = aligned(c, COLS)
     other_cols = aligned(other, COLS)
-    own_rows = aligned(c, ROWS)
-    other_rows = aligned(other, ROWS)
+    own_rows = aligned(half, ROWS)
+    other_rows = aligned(1 - half, ROWS)
 
     local = []
 
@@ -137,7 +144,7 @@
             yy, xx = y + along, x + across
         index = ((yy + SIDE) % SIDE) * SIDE + (xx + SIDE) % SIDE
         ref = w_all.at[l, pl.ds(pl.multiple_of(index * 256 + lo, 32), size), lanes(what, c)]
-        slot = group * 4 + (2 if fwd else 0) + (0 if sign == 1 else 1)
+        slot = group * 2 + (1 if fwd else 0)
         device = at_x(sign) if axis == 0 else at_y(sign)
         return rdma(ref, ref, sent.at[0], w_r.at[carrier % 3, slot], device)
 
@@ -151,16 +158,19 @@
         for sign in (1, -1):
             start(w_copy(carrier, group, half, axis, across, sign, False, True))
 
+    def w_wait(carrier, group, fwd):
+        l, what, _, size = carriers[carrier]
+        ref = w_all.at[l, pl.ds(0, size if fwd else 2 * size), lanes(what, c)]
+        rdma(ref, ref, sent.at[0], w_r.at[carrier % 3, group * 2 + (1 if fwd else 0)], partner).wait_recv()
+
     def w_forward(carrier, *name):
         group, half, axis, across = groups[name]
+        w_wait(carrier, group, False)
         for sign in (1, -1):
-            w_copy(carrier, group, half, axis, across, sign, False, False).wait_recv()
             start(w_copy(carrier, group, half, axis, across, sign, True, True))
 
     def w_finish(carrier, *name):
-        group, half, axis, across = groups[name]
-        for sign in (1, -1):
-            w_copy(carrier, group, half, axis, across, sign, True, False).wait_recv()
+        w_wait(carrier, groups[name][0], True)
 
     parcels = ((0, "proj"), (0, "out"), (1, "both"))
 
@@ -194,9 +204,9 @@
             for p in (-1, 1):
                 w_send(t, "a", 2, p)
                 w_send(t, "b", 2, p)
-        elif stage == 2:
             w_forward(t, "b", 2, 0)
             w_forward(t, "a", 2, 0)
+        elif stage == 2:
             w_finish(t, "a", 1)
             w_send(t, "a", 2, 2)
             w_finish(t, "b", 1)
@@ -205,17 +215,17 @@
             for p in (-1, 1):
                 w_forward(t, "a", 2, p)
                 w_forward(t, "b", 2, p)
-            w_finish(t, "a", 2, 0)
-            w_finish(t, "b", 2, 0)
-        elif stage == 4:
+        else:
             w_forward(t, "a", 2, 2)
             w_forward(t, "b", 2, 2)
-            for p in (-1, 1):
-                w_finish(t, "a", 2, p)
-                w_finish(t, "b", 2, p)
-        else:
-            w_finish(t, "a", 2, 2)
-            w_finish(t, "b", 2, 2)
+
+    def w_end(parcel, *ks):
+        with jax.named_scope(f"end#p={parcel}#k={ks[0]}"):
+            for k in ks:
+                for t in ((0, 1), (2,), (3,))[parcel]:
+                    w_finish(t, "a", 2, k)
+                    w_finish(t, "b", 2, k)
+        w_hand(parcel, *ks)
 
     def build_w_out(l, k):
         first = ((y + k + SIDE) % SIDE) * 8
@@ -232,45 +242,40 @@
     def chunk_at(k):
         return (z + k + NZ) % NZ
 
-    def ag_copy(l, way, dist, unit, sending):
+    def ag_copy(l, way, dist, unit):
         sign = 1 - 2 * way
         lo, size = GATHER[l][unit]
-        ref = x_all.at[l, chunk_at(-sign * (dist if sending else dist + 1)), pl.ds(lo, size), :]
-        slot = dist * 4 + unit
-        return rdma(ref, ref, sent.at[2], ag_r.at[way, slot], at_z(sign))
-
-    def first_copy(way, unit, crossing, sending):
-        sign = 1 - 2 * way
+        ref = x_all.at[l, chunk_at(-sign * dist), pl.ds(lo, size), :]
+        return rdma(ref, ref, sent.at[2], ag_r.at[dist * UNITS + unit], at_z(sign))
+
+    def first_copy(way, unit, crossing):
         lo, size = GATHER[0][unit]
-        cols = own_cols if sending or not crossing else other_cols
-        dst = x_all.at[0, z if sending else chunk_at(-sign), pl.ds(lo, size), cols]
-        src = res_other.at[pl.ds(lo, size), :] if crossing else x_all.at[0, z, pl.ds(lo, size), own_cols]
-        slot = unit * 2 + (1 if crossing else 0)
-        return rdma(src, dst, sent.at[2], ag0_r.at[way, slot], at_z(sign, other if crossing else c))
+        dst = x_all.at[0, z, pl.ds(lo, size), own_cols]
+        src = res_other.at[pl.ds(lo, size), :] if crossing else dst
+        return rdma(src, dst, sent.at[2], ag_r.at[unit], at_z(1 - 2 * way, other if crossing else c))
 
     def ag_first(l, unit):
         for way in range(2):
             if l == 0:
-                start(first_copy(way, unit, False, True))
-                start(first_copy(way, unit, True, True))
+                start(first_copy(way, unit, False))
+                start(first_copy(way, unit, True))
             else:
-                start(ag_copy(l, way, 0, unit, True))
+                start(ag_copy(l, way, 0, unit))
 
     def ag_step(l, dist, unit):
         with jax.named_scope(f"ag#l={l}#d={dist}#u={unit}"):
+            _, size = GATHER[l][unit]
+            ref = x_all.at[l, 0, pl.ds(0, size if dist == 3 else 2 * size), :]
+            rdma(ref, ref, sent.at[2], ag_r.at[dist * UNITS + unit], partner).wait_recv()
             for way in range(2):
-                if not has(way, dist == 3, unit):
-                    continue
-                if l == 0 and dist == 0:
-                    first_copy(way, unit, False, False).wait_recv()
-                    first_copy(way, unit, True, False).wait_recv()
-                else:
-                    ag_copy(l, way, dist, unit, False).wait_recv()
                 if dist < 3 and has(way, dist == 2, unit):
-                    start(ag_copy(l, way, dist + 1, unit, True))
+                    start(ag_copy(l, way, dist + 1, unit))
 
     def take(l, group, chunk):
-        lo, size = span(GATHER[l], group)
+        take_rows(l, span(GATHER[l], group), chunk)
+
+    def take_rows(l, which, chunk):
+        lo, size = which
         rows = pl.ds(lo, size)
         value = x_all[l, chunk, rows, :].astype(F32)
         square = value * value
@@ -284,7 +289,10 @@
         return (-dist - 1, dist + 1) if dist < 3 else (4,)
 
     def multiply(l, group, chunk):
-        lo, size = span(GATHER[l], group)
+        multiply_rows(l, span(GATHER[l], group), chunk)
+
+    def multiply_rows(l, which, chunk):
+        lo, size = which
         acc[lo : lo + size, :] += jnp.dot(
             xg[chunk, lo : lo + size, :],
             w_all[l, aligned(chunk, PIECE), CH : 7 * CH],
@@ -302,7 +310,10 @@
         acc[...] = jnp.zeros_like(acc)
 
     def gates(l, group):
-        lo, size = span(GATHER[l], group)
+        gates_rows(l, span(GATHER[l], group))
+
+    def gates_rows(l, which):
+        lo, size = which
         rows = pl.ds(lo, size)
         mean = jnp.sum(sq[rows, :], axis=1, keepdims=True) / D
         scale = lax.rsqrt(mean + FLOOR)
@@ -334,30 +345,35 @@
     def take_halo(l):
         with jax.named_scope("halo"):
             halo_copy(l).wait_recv()
-        first = jnp.logical_and(s == 0, c == 0)
+        first = jnp.logical_and(s == 0, half == 0)
         prod[:8, :] = jnp.where(first, 0.0, halo[l, 1])
 
-    def rs_copy(l, way, k, unit):
+    def rs_copy(l, i, way, k, unit):
         lo, size = REDUCE[l][unit]
         rows = pl.ds(lo, size)
-        slot = (k - 1) * 4 + unit
         return rdma(
             rs_out.at[l, way, k - 1, rows, :], rs_in.at[l, way, k - 1, rows, :],
-            sent.at[3], rs_r.at[way, slot], at_z(1 - 2 * way),
+            sent.at[3], rs_r.at[i * UNITS + unit], at_z(1 - 2 * way),
         )
 
     def partial(l, unit, chunk):
         lo, size = REDUCE[l][unit]
         return jnp.dot(mixed[lo : lo + size, :], w_out[:, aligned(chunk, PIECE)], preferred_element_type=F32)
 
+    def rs_wait(l, i, unit):
+        _, size = REDUCE[l][unit]
+        ref = rs_in.at[l, 0, 0, pl.ds(0, size if i == 3 else 2 * size), :]
+        rdma(ref, ref, sent.at[3], rs_r.at[i * UNITS + unit], partner).wait_recv()
+
     def arrived(l, way, k, unit):
-        rs_copy(l, way, k, unit).wait_recv()
         lo, size = REDUCE[l][unit]
         return rs_in[l, way, k - 1, lo : lo + size, :].astype(F32)
 
     def rs_step(l, i, unit):
         with jax.named_scope(f"rs#l={l}#i={i}#u={unit}"):
             lo, size = REDUCE[l][unit]
+            if i > 0:
+                rs_wait(l, i - 1, unit)
             for way in range(2):
                 k = 4 - i if has(way, True, unit) else 3 - i
                 if k < 1:
@@ -366,12 +382,13 @@
                 if i > 0:
                     value = value + arrived(l, way, k + 1, unit)
                 rs_out[l, way, k - 1, lo : lo + size, :] = value.astype(BF16)
-                start(rs_copy(l, way, k, unit))
+                start(rs_copy(l, i, way, k, unit))
 
     def rs_last(l, unit):
         with jax.named_scope(f"last#l={l}#u={unit}"):
             lo, size = REDUCE[l][unit]
             value = partial(l, unit, z)
+            rs_wait(l, 3, unit)
             for way in range(2):
                 value = value + arrived(l, way, 1, unit)
             return (x_all[l, z, lo : lo + size, :].astype(F32) + value).astype(BF16)
@@ -388,8 +405,8 @@
     w_stage(1, 0)
     start(rdma(res_other, x_all.at[0, z, :, own_cols], sent.at[4], m_r.at[0], partner))
     start(rdma(tap_all.at[c], tap_all.at[c], sent.at[5], m_r.at[1], partner))
-    ag_first(0, 2)
-    ag_first(0, 3)
+    for unit in (3, 4, 2):
+        ag_first(0, unit)
     start_sums()
     rdma(res_other, x_all.at[0, z, :, other_cols], sent.at[4], m_r.at[0], partner).wait_recv()
     take(0, 0, z)
@@ -401,53 +418,49 @@
     w_stage(1, 1)
     ag_step(0, 0, 1)
     take_step(0, 0, 0)
+    ag_step(0, 0, 3)
+    ag_step(0, 0, 4)
+    w_stage(0, 2)
     ag_step(0, 0, 2)
-    ag_step(0, 0, 3)
     take_step(0, 1, 0)
     w_stage(2, 1)
-    w_stage(0, 2)
+    w_stage(1, 2)
     ag_step(0, 1, 0)
-    w_stage(1, 2)
+    w_stage(0, 3)
     ag_step(0, 1, 1)
     take_step(0, 0, 1)
-    ag_step(0, 1, 2)
-    w_stage(0, 3)
-    ag_step(0, 1, 3)
-    take_step(0, 1, 1)
     w_stage(2, 2)
     w_stage(1, 3)
-    w_hand(0, 0)
+    ag_step(0, 1, 3)
+    ag_step(0, 1, 4)
+    w_stage(0, 4)
+    ag_step(0, 1, 2)
+    take_step(0, 1, 1)
+    w_stage(1, 4)
+    w_stage(2, 3)
+    w_end(0, 0)
     ag_step(0, 2, 0)
-    w_stage(0, 4)
+    w_stage(2, 4)
     ag_step(0, 2, 1)
     take_step(0, 0, 2)
-    w_stage(2, 3)
-    w_stage(1, 4)
-    w_hand(0, -1, 1)
-    w_hand(1, 0)
+    w_end(0, -1, 1)
+    w_end(1, 0)
+    ag_step(0, 2, 3)
+    ag_step(0, 2, 4)
+    w_end(0, 2)
     ag_step(0, 2, 2)
-    ag_step(0, 2, 3)
     take_step(0, 1, 2)
-    w_stage(0, 5)
-    w_stage(2, 4)
-    w_hand(1, -1, 1)
+    w_end(1, -1, 1)
     ag_step(0, 3, 0)
     ag_step(0, 3, 1)
     take_step(0, 0, 3)
-    w_stage(1, 5)
-    w_hand(0, 2)
-    w_taken(0, 0)
-    multiply_row(0, 0, 0)
-    w_taken(0, -1)
-    multiply_row(0, 0, -1)
-    w_stage(2, 5)
-    w_hand(1, 2)
+    w_end(1, 2)
     w_stage(3, 0)
-    for k in (1, 2):
+    for k in (0, -1, 1, 2):
         w_taken(0, k)
         multiply_row(0, 0, k)
-    ag_step(0, 3, 2)
-    ag_step(0, 3, 3)
+    for unit in (3, 4, 2):
+        ag_step(0, 3, unit)
     take_step(0, 1, 3)
     gates(0, 0)
     rdma(tap_all.at[other], tap_all.at[other], sent.at[4], m_r.at[1], partner).wait_recv()
@@ -458,102 +471,105 @@
         w_taken(1, k)
         build_w_out(0, k)
 
+    rs_step(0, 0, 0)
     rs_step(0, 0, 1)
-    rs_step(0, 0, 0)
     for k in (0, -1, 1, 2):
         multiply_row(0, 1, k)
     gates(0, 1)
-    mix(0, 3)
-    rs_step(0, 0, 3)
-    rs_step(0, 1, 1)
+    for unit in (3, 4):
+        mix(0, unit)
+        rs_step(0, 0, unit)
+    rs_step(0, 1, 0)
     take_halo(0)
     mix(0, 2)
     rs_step(0, 0, 2)
     start_sums()
-    rs_step(0, 1, 0)
-    rs_step(0, 1, 3)
+    for unit in (1, 3, 4):
+        rs_step(0, 1, unit)
     w_stage(3, 1)
-    rs_step(0, 2, 1)
+    rs_step(0, 2, 0)
     rs_step(0, 1, 2)
-    rs_step(0, 2, 0)
-    rs_step(0, 2, 3)
+    for unit in (1, 3, 4):
+        rs_step(0, 2, unit)
+    rs_step(0, 3, 0)
+    rs_step(0, 2, 2)
     w_stage(3, 2)
-    rs_step(0, 3, 1)
-    rs_step(0, 2, 2)
-    rs_step(0, 3, 0)
-    rs_step(0, 3, 3)
-    w_stage(3, 3)
-    w_hand(2, 0)
+    for unit in (1, 3, 4):
+        rs_step(0, 3, unit)
 
     def next_stream(unit):
         lo, size = REDUCE[0][unit]
         x_all[1, z, lo : lo + size, :] = rs_last(0, unit)
         ag_first(1, unit)
 
+    next_stream(0)
+    rs_step(0, 3, 2)
+    w_stage(3, 3)
     next_stream(1)
-    rs_step(0, 3, 2)
-    next_stream(0)
     take(1, 0, z)
     next_stream(3)
+    next_stream(4)
+
+    ag_step(1, 0, 0)
+    w_stage(3, 4)
     next_stream(2)
     take(1, 1, z)
-
     ag_step(1, 0, 1)
-    ag_step(1, 0, 0)
-    w_stage(3, 4)
-    w_hand(2, -1, 1)
     ag_step(1, 0, 3)
+    w_end(2, 0)
+    w_end(2, -1, 1)
+    ag_step(1, 0, 4)
     ag_step(1, 0, 2)
+    ag_step(1, 1, 0)
     ag_step(1, 1, 1)
-    ag_step(1, 1, 0)
-    w_stage(3, 5)
-    w_hand(2, 2)
-    ag_step(1, 1, 3)
-    ag_step(1, 1, 2)
+    w_end(2, 2)
+    for unit in (3, 4, 2):
+        ag_step(1, 1, unit)
     for k in (0, -1, 1, 2):
         w_taken(2, k)
         build_w_out(1, k)
-    ag_step(1, 2, 1)
+    ag_step(1, 2, 0)
     for group in range(2):
         multiply(1, group, z)
         take_step(1, group, 0)
-    ag_step(1, 2, 0)
+    ag_step(1, 2, 1)
     take_step(1, 0, 1)
     ag_step(1, 2, 3)
     take_step(1, 1, 1)
+    ag_step(1, 2, 4)
     ag_step(1, 2, 2)
     take_step(1, 0, 2)
     take_step(1, 1, 2)
-    ag_step(1, 3, 1)
-    ag_step(1, 3, 0)
-    take_step(1, 0, 3)
-    gates(1, 0)
-    give_halo(1)
-    mix(1, 1)
-    mix(1, 0)
-    rs_step(1, 0, 1)
-    rs_step(1, 0, 0)
-    ag_step(1, 3, 3)
-    ag_step(1, 3, 2)
+    for unit in (0, 1):
+        ag_step(1, 3, unit)
+        take_rows(1, GATHER[1][unit], chunk_at(4))
+        multiply_rows(1, GATHER[1][unit], chunk_at(4))
+        gates_rows(1, GATHER[1][unit])
+        if unit == 1:
+            give_halo(1)
+        mix(1, unit)
+        rs_step(1, 0, unit)
+    for unit in (3, 4, 2):
+        ag_step(1, 3, unit)
     take_step(1, 1, 3)
     gates(1, 1)
-    mix(1, 3)
-    rs_step(1, 0, 3)
-    rs_step(1, 1, 1)
+    for unit in (3, 4):
+        mix(1, unit)
+        rs_step(1, 0, unit)
+    rs_step(1, 1, 0)
     take_halo(1)
     mix(1, 2)
     rs_step(1, 0, 2)
-    rs_step(1, 1, 0)
-    rs_step(1, 1, 3)
-    rs_step(1, 2, 1)
+    for unit in (1, 3, 4):
+        rs_step(1, 1, unit)
+    rs_step(1, 2, 0)
     rs_step(1, 1, 2)
-    rs_step(1, 2, 0)
-    rs_step(1, 2, 3)
-    rs_step(1, 3, 1)
+    for unit in (1, 3, 4):
+        rs_step(1, 2, unit)
+    rs_step(1, 3, 0)
     rs_step(1, 2, 2)
-    rs_step(1, 3, 0)
-    rs_step(1, 3, 3)
-    rs_step(1, 3, 2)
+    for unit in (1, 3, 4, 2):
+        rs_step(1, 3, unit)
 
     def fin_copy(group):
         rows = pl.ds(*span(REDUCE[1], group))
@@ -566,7 +582,7 @@
     routes = [(4, 0), (4, 1), (3, 0), (3, 1), (5, 0), (5, 1), (2, 0), (2, 1), (6, 0), (6, 1)]
     routes += [(1, 0), (1, 1), (7, 0), (7, 1), (0, 1)]
     for group in range(2):
-        for unit in GROUPS[group]:
+        for unit in ((0, 1), (3, 4, 2))[group]:
             lo, size = REDUCE[1][unit]
             st[lo : lo + size, :] = rs_last(1, unit).astype(F32)
         lo, size = span(REDUCE[1], group)
@@ -627,11 +643,10 @@
             pltpu.VMEM((ROWS, COLS), BF16),
             dma((1,)),
             dma((6,)),
-            dma((2, 8)),
-            dma((2, 16)),
-            dma((3, 40)),
+            dma((4 * UNITS,)),
+            dma((3, 20)),
             dma((3, SIDE)),
-            dma((2, 16)),
+            dma((4 * UNITS,)),
             dma((LAYERS,)),
             dma((2, 2)),
             dma((4,)),

time: 111 us -> 111 us (level)
  no operation moved by 1% of the time
where the time goes in v4:
time: 111 us
  Pallas kernels  110 us (99%)
    pallas_call x1, Pallas kernels, per_device(): pl.pallas_call(kernel, out_shape=jax.ShapeDtypeStruct((2 * ROWS, COLS), F...  110 us

profile of v4, /device:TPU:1, one launch (start us, length us, event | category | flops | bytes accessed | tf_op | source)
XLA Modules:
  0.0 111.2 jit_solution(4315714731908637318)
XLA Ops:
  0.0 110.4 %shard_map.82 = f32[512,256]{1,0:T(8,128)S(1)} custom-call(bf16[512,256]{1,0:T(8,128)(2,1)} %res.1, f32[2,4096]{1,0:T(2,128)} %norm_gain.1, bf16[2,256,128]{2,1,0:T(8,128)(2,1)} %gate.1, bf16[2,256,128]{2,1,0:T(8,128)(2,1)} %filt.1, bf16[2,256,128]{2,1,0:T(8,128)(2,1)} %sig.1, f32[3,2,128]{2,1,0:T(2,128)} %bitcast.2, bf16[2,128,256]{2,1,0:T(8,128)(2,1)} %outp.1, ...), custom_call_target="tpu_custom_call" | custom-call | tf_op jit(solution)/shard_map/pallas_call | solution.py:619
  110.4 0.8 copy.10

commit v5 on v4

--- a/solution.py
+++ b/solution.py
@@ -424,52 +424,61 @@
     ag_step(0, 0, 2)
     take_step(0, 1, 0)
     w_stage(2, 1)
+    ag_step(0, 1, 0)
     w_stage(1, 2)
-    ag_step(0, 1, 0)
     w_stage(0, 3)
     ag_step(0, 1, 1)
     take_step(0, 0, 1)
-    w_stage(2, 2)
-    w_stage(1, 3)
     ag_step(0, 1, 3)
     ag_step(0, 1, 4)
-    w_stage(0, 4)
+    w_stage(1, 3)
     ag_step(0, 1, 2)
     take_step(0, 1, 1)
-    w_stage(1, 4)
-    w_stage(2, 3)
-    w_end(0, 0)
+    w_stage(0, 4)
     ag_step(0, 2, 0)
-    w_stage(2, 4)
     ag_step(0, 2, 1)
     take_step(0, 0, 2)
-    w_end(0, -1, 1)
-    w_end(1, 0)
+    w_stage(2, 2)
+    w_stage(1, 4)
     ag_step(0, 2, 3)
     ag_step(0, 2, 4)
-    w_end(0, 2)
+    w_end(0, 0)
+    w_stage(2, 3)
     ag_step(0, 2, 2)
     take_step(0, 1, 2)
-    w_end(1, -1, 1)
+    w_end(0, -1, 1)
     ag_step(0, 3, 0)
+    w_stage(2, 4)
+    w_end(1, 0)
     ag_step(0, 3, 1)
     take_step(0, 0, 3)
-    w_end(1, 2)
-    w_stage(3, 0)
-    for k in (0, -1, 1, 2):
-        w_taken(0, k)
-        multiply_row(0, 0, k)
+    w_end(0, 2)
+    w_taken(0, 0)
+    multiply_row(0, 0, 0)
     for unit in (3, 4, 2):
         ag_step(0, 3, unit)
     take_step(0, 1, 3)
+    w_end(1, -1, 1)
+    w_taken(0, -1)
+    multiply_row(0, 0, -1)
+    w_taken(1, 0)
+    build_w_out(0, 0)
+    w_end(1, 2)
+    w_stage(3, 0)
+    w_taken(0, 1)
+    multiply_row(0, 0, 1)
+    for k in (-1, 1):
+        w_taken(1, k)
+        build_w_out(0, k)
+    w_taken(0, 2)
+    multiply_row(0, 0, 2)
     gates(0, 0)
     rdma(tap_all.at[other], tap_all.at[other], sent.at[4], m_r.at[1], partner).wait_recv()
     give_halo(0)
+    mix(0, 0)
     mix(0, 1)
-    mix(0, 0)
-    for k in (0, -1, 1, 2):
-        w_taken(1, k)
-        build_w_out(0, k)
+    w_taken(1, 2)
+    build_w_out(0, 2)
 
     rs_step(0, 0, 0)
     rs_step(0, 0, 1)

time: 111 us -> 110 us (level)
  no operation moved by 1% of the time
where the time goes in v5:
time: 110 us
  Pallas kernels  110 us (100%)
    pallas_call x1, Pallas kernels, per_device(): pl.pallas_call(kernel, out_shape=jax.ShapeDtypeStruct((2 * ROWS, COLS), F...  110 us

profile of v5, /device:TPU:1, one launch (start us, length us, event | category | flops | bytes accessed | tf_op | source)
XLA Modules:
  0.0 110.4 jit_solution(4489331606365418450)
XLA Ops:
  0.0 109.6 %shard_map.82 = f32[512,256]{1,0:T(8,128)S(1)} custom-call(bf16[512,256]{1,0:T(8,128)(2,1)} %res.1, f32[2,4096]{1,0:T(2,128)} %norm_gain.1, bf16[2,256,128]{2,1,0:T(8,128)(2,1)} %gate.1, bf16[2,256,128]{2,1,0:T(8,128)(2,1)} %filt.1, bf16[2,256,128]{2,1,0:T(8,128)(2,1)} %sig.1, f32[3,2,128]{2,1,0:T(2,128)} %bitcast.2, bf16[2,128,256]{2,1,0:T(8,128)(2,1)} %outp.1, ...), custom_call_target="tpu_custom_call" | custom-call | tf_op jit(solution)/shard_map/pallas_call | solution.py:628
  109.6 0.8 copy.10

commit v6 on v5

--- a/solution.py
+++ b/solution.py
@@ -54,7 +54,7 @@
     res, norm_gain, gate, filt, sig, taps, outp, final_gain, out,
     x_all, res_other, xg, w_all, w_out, acc, prod, mixed, sq, rs_out, rs_in, halo, tap_all, gain_in, gain_out,
     sums, st, fin_out, fin_in,
-    loc, sent, ag_r, w_r, d_r, rs_r, h_r, s_r, m_r,
+    loc, sent, ring_r, w_r, d_r, h_r, s_r, m_r,
 ):
     s = lax.axis_index("sp")
     t = lax.axis_index("tp")
@@ -246,13 +246,13 @@
         sign = 1 - 2 * way
         lo, size = GATHER[l][unit]
         ref = x_all.at[l, chunk_at(-sign * dist), pl.ds(lo, size), :]
-        return rdma(ref, ref, sent.at[2], ag_r.at[dist * UNITS + unit], at_z(sign))
+        return rdma(ref, ref, sent.at[2], ring_r.at[dist * UNITS + unit], at_z(sign))
 
     def first_copy(way, unit, crossing):
         lo, size = GATHER[0][unit]
         dst = x_all.at[0, z, pl.ds(lo, size), own_cols]
         src = res_other.at[pl.ds(lo, size), :] if crossing else dst
-        return rdma(src, dst, sent.at[2], ag_r.at[unit], at_z(1 - 2 * way, other if crossing else c))
+        return rdma(src, dst, sent.at[2], ring_r.at[unit], at_z(1 - 2 * way, other if crossing else c))
 
     def ag_first(l, unit):
         for way in range(2):
@@ -266,7 +266,7 @@
         with jax.named_scope(f"ag#l={l}#d={dist}#u={unit}"):
             _, size = GATHER[l][unit]
             ref = x_all.at[l, 0, pl.ds(0, size if dist == 3 else 2 * size), :]
-            rdma(ref, ref, sent.at[2], ag_r.at[dist * UNITS + unit], partner).wait_recv()
+            rdma(ref, ref, sent.at[2], ring_r.at[dist * UNITS + unit], partner).wait_recv()
             for way in range(2):
                 if dist < 3 and has(way, dist == 2, unit):
                     start(ag_copy(l, way, dist + 1, unit))
@@ -353,7 +353,7 @@
         rows = pl.ds(lo, size)
         return rdma(
             rs_out.at[l, way, k - 1, rows, :], rs_in.at[l, way, k - 1, rows, :],
-            sent.at[3], rs_r.at[i * UNITS + unit], at_z(1 - 2 * way),
+            sent.at[3], ring_r.at[i * UNITS + unit], at_z(1 - 2 * way),
         )
 
     def partial(l, unit, chunk):
@@ -363,7 +363,7 @@
     def rs_wait(l, i, unit):
         _, size = REDUCE[l][unit]
         ref = rs_in.at[l, 0, 0, pl.ds(0, size if i == 3 else 2 * size), :]
-        rdma(ref, ref, sent.at[3], rs_r.at[i * UNITS + unit], partner).wait_recv()
+        rdma(ref, ref, sent.at[3], ring_r.at[i * UNITS + unit], partner).wait_recv()
 
     def arrived(l, way, k, unit):
         lo, size = REDUCE[l][unit]
@@ -372,13 +372,12 @@
     def rs_step(l, i, unit):
         with jax.named_scope(f"rs#l={l}#i={i}#u={unit}"):
             lo, size = REDUCE[l][unit]
+            moves = [(way, 4 - i if has(way, True, unit) else 3 - i) for way in range(2)]
+            moves = [(way, k) for way, k in moves if k > 0]
+            values = [partial(l, unit, chunk_at(k * (1 - 2 * way))) for way, k in moves]
             if i > 0:
                 rs_wait(l, i - 1, unit)
-            for way in range(2):
-                k = 4 - i if has(way, True, unit) else 3 - i
-                if k < 1:
-                    continue
-                value = partial(l, unit, chunk_at(k * (1 - 2 * way)))
+            for (way, k), value in zip(moves, values):
                 if i > 0:
                     value = value + arrived(l, way, k + 1, unit)
                 rs_out[l, way, k - 1, lo : lo + size, :] = value.astype(BF16)
@@ -655,7 +654,6 @@
             dma((4 * UNITS,)),
             dma((3, 20)),
             dma((3, SIDE)),
-            dma((4 * UNITS,)),
             dma((LAYERS,)),
             dma((2, 2)),
             dma((4,)),

time: 110 us -> 110 us (level)
  no operation moved by 1% of the time
where the time goes in v6:
time: 110 us
  Pallas kernels  109 us (99%)
    pallas_call x1, Pallas kernels, per_device(): pl.pallas_call(kernel, out_shape=jax.ShapeDtypeStruct((2 * ROWS, COLS), F...  109 us

profile of v6, /device:TPU:1, one launch (start us, length us, event | category | flops | bytes accessed | tf_op | source)
XLA Modules:
  0.0 110.0 jit_solution(4362198182141126658)
XLA Ops:
  0.0 109.2 %shard_map.82 = f32[512,256]{1,0:T(8,128)S(1)} custom-call(bf16[512,256]{1,0:T(8,128)(2,1)} %res.1, f32[2,4096]{1,0:T(2,128)} %norm_gain.1, bf16[2,256,128]{2,1,0:T(8,128)(2,1)} %gate.1, bf16[2,256,128]{2,1,0:T(8,128)(2,1)} %filt.1, bf16[2,256,128]{2,1,0:T(8,128)(2,1)} %sig.1, f32[3,2,128]{2,1,0:T(2,128)} %bitcast.2, bf16[2,128,256]{2,1,0:T(8,128)(2,1)} %outp.1, ...), custom_call_target="tpu_custom_call" | custom-call | tf_op jit(solution)/shard_map/pallas_call | solution.py:627
  109.2 0.8 copy.10

commit v7 on v6

--- a/solution.py
+++ b/solution.py
@@ -607,14 +607,17 @@
         total = jnp.sum(sums[core, :, 0, :], axis=0, keepdims=True)
         return lax.rsqrt(jnp.broadcast_to(total, (128, ROWS)).T[:, :1] / D + FLOOR)
 
+    out[own_rows, :] = st[:, own_cols] * gain_out[...]
     with jax.named_scope("sums"):
         for group in range(2):
             fin_copy(group).wait_recv()
+        out[other_rows, :] = fin_in[...].astype(F32) * gain_out[...]
+        for group in range(2):
             cols = pl.ds(*span(REDUCE[1], group))
             for crossing, ref in enumerate((sums.at[c, pl.ds(0, NZ - 1), :, cols], sums.at[other, :, :, cols])):
                 rdma(ref, ref, sent.at[4], s_r.at[group, crossing], partner).wait_recv()
-    out[own_rows, :] = st[:, own_cols] * scale_of(c) * gain_out[...]
-    out[other_rows, :] = fin_in[...].astype(F32) * scale_of(other) * gain_out[...]
+    out[own_rows, :] = out[own_rows, :] * scale_of(c)
+    out[other_rows, :] = out[other_rows, :] * scale_of(other)
     with jax.named_scope("sends"):
         for kind, rows in enumerate(SENT_ROWS):
             ref = w_all.at[0, pl.ds(0, rows), pl.ds(0, WIDE)] if rows <= D else w_all.at[0, pl.ds(0, rows // 2), :]

time: 110 us -> 110 us (level)
  no operation moved by 1% of the time
where the time goes in v7:
time: 110 us
  Pallas kernels  109 us (99%)
    pallas_call x1, Pallas kernels, per_device(): pl.pallas_call(kernel, out_shape=jax.ShapeDtypeStruct((2 * ROWS, COLS), F...  109 us

profile of v7, /device:TPU:1, one launch (start us, length us, event | category | flops | bytes accessed | tf_op | source)
XLA Modules:
  0.0 110.0 jit_solution(18111631278638588074)
XLA Ops:
  0.0 109.2 %shard_map.82 = f32[512,256]{1,0:T(8,128)S(1)} custom-call(bf16[512,256]{1,0:T(8,128)(2,1)} %res.1, f32[2,4096]{1,0:T(2,128)} %norm_gain.1, bf16[2,256,128]{2,1,0:T(8,128)(2,1)} %gate.1, bf16[2,256,128]{2,1,0:T(8,128)(2,1)} %filt.1, bf16[2,256,128]{2,1,0:T(8,128)(2,1)} %sig.1, f32[3,2,128]{2,1,0:T(2,128)} %bitcast.2, bf16[2,128,256]{2,1,0:T(8,128)(2,1)} %outp.1, ...), custom_call_target="tpu_custom_call" | custom-call | tf_op jit(solution)/shard_map/pallas_call | solution.py:630
  109.2 0.8 copy.10
